TPU v7x, 256 devices: a whole 4x4x8 slice. The times are simulated.
256 devices in a mesh: ra: 2 (over core), cb: 32 (over z, x), dp: 4 (over y).
Axes of the slice: x: 4, y: 4, z: 8, core: 2. Of those that a mesh axis runs over, the one named last changes fastest.
Arguments:
- residual_in: bfloat16 [1024, 4096], P('dp', 'cb'), may hold values from -220 to 220, as said below
- gain_in: float32 [4096], P('cb'), may hold values from 0.1 to 1.9
- shift_in: float32 [4096], P('cb'), may hold values from -3 to 3
- up_weight: bfloat16 [4096, 16384], P('cb', 'ra'), may hold values from -0.09375 to 0.09375
- down_weight: bfloat16 [16384, 4096], P('ra', 'cb'), may hold values from -0.046875 to 0.046875
- gain_out: float32 [4096], P('cb'), may hold values from 0.1 to 1.9
- shift_out: float32 [4096], P('cb'), may hold values from -3 to 3
Outputs:
- layer_out: bfloat16 [1024, 4096], P('dp', 'cb')
Inputs may be any that keep to these rules, and one draw needn't show every extreme that they name: `residual_in`: real-valued activations.
All inputs are finite; a program needn't handle non-finite values.
Results may differ from a plain program's by a relative error of at most 0.0065.
Values may be sent and summed in bfloat16 or wider, within the bound.
A program may use at most 64 MiB of HBM per device.

v0:
```python
import jax
import jax.numpy as jnp
from jax import lax
from jax.sharding import Mesh
from jax.sharding import PartitionSpec as P

CB = ("cb_0", "cb_1")


def from_everyone(shard, axis):
    copies = jnp.broadcast_to(shard, (lax.axis_size(axis), *shard.shape))
    return lax.all_to_all(copies, axis, split_axis=0, concat_axis=0, tiled=True)


def of_everyone(shard, axis):
    everything = from_everyone(shard, axis)
    return jnp.sum(everything, axis=0)


def in_one(arrays, axis):
    ends = [0]
    for a in arrays:
        ends.append(ends[-1] + a.size)
    running = of_everyone(jnp.concatenate([a.ravel() for a in arrays]), axis)
    return tuple((running[b:e].reshape(a.shape) for a, b, e in zip(arrays, ends, ends[1:])))


def scatter_axes(shard, axes, dim):
    if not axes:
        return shard
    nearer = lax.psum_scatter(shard, axes[0], scatter_dimension=dim, tiled=True)
    return scatter_axes(nearer, axes[1:], dim)


def whole_of(shard, axes, dim):
    for axis in reversed(axes):
        shard = lax.all_gather(shard, axis, axis=dim, tiled=True)
    return shard


def standardize(values):
    count = values.shape[1] * lax.axis_size(CB)
    sums, squares = in_one((jnp.sum(values, axis=1), jnp.sum(values * values, axis=1)), CB)
    mean = sums / count
    spread = squares / count - mean * mean
    return (values - mean[:, None]) * lax.rsqrt(spread + 1e-05)[:, None]


def per_device(residual_in, gain_in, shift_in, up_weight, down_weight, gain_out, shift_out):
    normed = (standardize(residual_in.astype(jnp.float32)) * gain_in + shift_in).astype(
        jnp.bfloat16
    )
    products = jnp.dot(normed, up_weight, preferred_element_type=jnp.float32)
    share = scatter_axes(products, CB, 1)
    hidden_share = jnp.square(jax.nn.relu(share)).astype(jnp.bfloat16)
    branch_part = jnp.dot(
        whole_of(hidden_share, CB, 1), down_weight, preferred_element_type=jnp.float32
    )
    branch = of_everyone(branch_part, "ra")
    total = 2.0**0.25 * normed.astype(jnp.float32) + branch
    return (standardize(total) * gain_out + shift_out).astype(jnp.bfloat16)


def solution(mesh):
    split = Mesh(
        mesh.devices.reshape(mesh.shape["ra"], 8, 4, mesh.shape["dp"]), ("ra", "cb_0", "cb_1", "dp")
    )
    placed = (P("dp", CB), P(CB), P(CB), P(CB, "ra"), P("ra", CB), P(CB), P(CB))
    return jax.shard_map(
        per_device, mesh=split, in_specs=placed, out_specs=P("dp", CB), check_vma=False
    )
```

profile of v0, /device:TPU:1, one launch (start us, length us, event | category | flops | bytes accessed | tf_op | source)
XLA Modules:
  0.0 253.7 jit_solution(1986165354663769400)
XLA Ops:
  6.5 0.0 copy-start
  6.5 0.0 reduce-scatter.3.cloned.1.call-start
  6.5 1.1 convert_reduce_fusion
  7.7 20.5 %all_to_all.17 = f32[32,1,512]{2,1,0:T(1,128)S(1)} all-to-all(f32[32,1,512]{2,1,0:T(1,128)S(1)} %broadcast_in_dim.6), channel_id=1, replica_groups=mesh['ra'=2,'cb_0'=8,'cb_1'=4,'dp'=4] {'cb_0','cb_1'}, dimensions={0} | all-to-all | bytes 131072 | tf_op jit(solution)/shard_map/all_to_all | solution.py:12
  28.2 0.1 reduce_sum.65
  28.3 0.0 copy-done
  28.3 5.4 %fusion.6 = f32[256,8192]{1,0:T(8,128)} fusion(bf16[128,8192]{1,0:T(8,128)(2,1)S(1)} %copy-done, bf16[256,128]{1,0:T(8,128)(2,1)} %param.7, f32[128]{0:T(128)} %param.9, f32[128]{0:T(128)} %param.8, f32[256]{0:T(256)S(1)} %get-tuple-element.12, f32[256]{0:T(256)S(1)} %get-tuple-element.11), kind=kOutput, calls=%fused_computation.19 | convolution fusion | flops 537067520 | bytes 10554368 | tf_op jit(solution)/shard_map/dot_general | solution.py:53
  33.7 0.0 reduce-scatter.3.cloned.1.call-update
  33.7 0.0 reduce-scatter.5.cloned.1.call-start
  33.8 91.4 %reduce-scatter.3.cloned.1.call-done = f32[256,1024]{1,0:T(8,128)} async-done(((f32[256,8192]{1,0:T(8,128)}), f32[256,1024]{1,0:T(8,128)}) %reduce-scatter.3.cloned.1.call-update) | async-done | bytes 1048592 | tf_op jit(solution)/shard_map/reduce_scatter | solution.py:31
  125.1 0.0 reduce-scatter.5.cloned.1.call-update
  125.1 0.0 all-gather.2.cloned.1.call-start
  125.2 26.0 %reduce-scatter.5.cloned.1.call-done = f32[256,256]{1,0:T(8,128)} async-done(((f32[256,1024]{1,0:T(8,128)}), f32[256,256]{1,0:T(8,128)}) %reduce-scatter.5.cloned.1.call-update) | async-done | bytes 262160 | tf_op jit(solution)/shard_map/reduce_scatter | solution.py:31
  151.2 1.0 multiply_convert_fusion
  152.2 11.0 %all_gather.6 = bf16[256,1024]{1,0:T(8,128)(2,1)} all-gather(bf16[256,256]{1,0:T(8,128)(2,1)S(1)} %multiply_convert_fusion), channel_id=1, replica_groups=mesh['ra'=2,'cb_0'=8,'cb_1'=4,'dp'=4] {'cb_1'}, dimensions={1}, use_global_device_ids=true | all-gather | bytes 655360 | tf_op jit(solution)/shard_map/all_gather | solution.py:37
  163.2 0.0 all-gather.2.cloned.1.call-update
  163.2 0.0 copy-start.1
  163.2 0.0 copy-start.2
  163.2 0.0 copy-start.3
  163.2 0.0 copy-start.4
  163.2 0.0 copy-start.5
  163.3 58.5 %all-gather.2.cloned.1.call-done = bf16[256,8192]{1,0:T(8,128)(2,1)} async-done(((bf16[256,1024]{1,0:T(8,128)(2,1)}), bf16[256,8192]{1,0:T(8,128)(2,1)}) %all-gather.2.cloned.1.call-update) | async-done | bytes 4194320 | tf_op jit(solution)/shard_map/all_gather | solution.py:37
  221.8 4.2 %fusion.8 = f32[256,128]{1,0:T(8,128)S(1)} fusion(bf16[256,8192]{1,0:T(8,128)(2,1)} %all-gather.2.cloned.1.call-done, bf16[8192,128]{1,0:T(8,128)(2,1)} %param.11), kind=kOutput, calls=%fused_computation.20 | convolution fusion | flops 536870912 | bytes 6422528 | tf_op jit(solution)/shard_map/dot_general | solution.py:56
  226.0 4.4 %all_to_all.18 = f32[2,256,128]{2,1,0:T(8,128)S(1)} all-to-all(f32[2,256,128]{2,1,0:T(8,128)S(1)} %broadcast_in_dim.7), channel_id=1, replica_groups=mesh['ra'=2,'cb_0'=8,'cb_1'=4,'dp'=4] {'ra'}, dimensions={0} | all-to-all | bytes 524288 | tf_op jit(solution)/shard_map/all_to_all | solution.py:12
  230.5 0.0 copy-done.1
  230.5 0.0 copy-done.2
  230.5 0.0 copy-done.3
  230.5 0.3 fusion.5
  230.8 15.5 %all_to_all.19 = f32[32,1,512]{2,1,0:T(1,128)S(1)} all-to-all(f32[32,1,512]{2,1,0:T(1,128)S(1)} %broadcast_in_dim.8), channel_id=1, replica_groups=mesh['ra'=2,'cb_0'=8,'cb_1'=4,'dp'=4] {'cb_0','cb_1'}, dimensions={0} | all-to-all | bytes 131072 | tf_op jit(solution)/shard_map/all_to_all | solution.py:12
  246.3 0.1 reduce_sum.69
  246.3 0.0 copy-done.4
  246.4 0.0 copy-done.5
  246.4 0.8 add_convert_fusion
  (8 shorter events, 0.2 us)
Async XLA Ops:
  6.5 21.8 %copy-start = (bf16[128,8192]{1,0:T(8,128)(2,1)S(1)}, bf16[128,8192]{1,0:T(8,128)(2,1)}, u32[]{:S(2)}) copy-start(bf16[128,8192]{1,0:T(8,128)(2,1)} %param.10) | copy-start | bytes 6291460
  6.5 118.6 %reduce-scatter.3.cloned.1.call-start = ((), (), s32[]{:S(2)}) async-start(), calls=%async_computation.5 | async-start | bytes 9437184 | tf_op jit(solution)/shard_map/reduce_scatter | solution.py:31
  33.7 117.5 %reduce-scatter.5.cloned.1.call-start = ((), (), s32[]{:S(2)}) async-start(), calls=%async_computation.6 | async-start | bytes 1310720 | tf_op jit(solution)/shard_map/reduce_scatter | solution.py:31
  125.1 96.7 %all-gather.2.cloned.1.call-start = ((), (), s32[]{:S(2)}) async-start(), calls=%async_computation.7 | async-start | bytes 4718592 | tf_op jit(solution)/shard_map/all_gather | solution.py:37
  163.2 67.3 %copy-start.1 = (bf16[256,128]{1,0:T(8,128)(2,1)S(1)}, bf16[256,128]{1,0:T(8,128)(2,1)}, u32[]{:S(2)}) copy-start(bf16[256,128]{1,0:T(8,128)(2,1)} %param.7) | copy-start | bytes 196612
  163.2 67.3 %copy-start.2 = (f32[128]{0:T(128)S(1)}, f32[128]{0:T(128)}, u32[]{:S(2)}) copy-start(f32[128]{0:T(128)} %param.9) | copy-start | bytes 1540
  163.2 67.3 %copy-start.3 = (f32[128]{0:T(128)S(1)}, f32[128]{0:T(128)}, u32[]{:S(2)}) copy-start(f32[128]{0:T(128)} %param.8) | copy-start | bytes 1540
  163.2 83.1 %copy-start.4 = (f32[128]{0:T(128)S(1)}, f32[128]{0:T(128)}, u32[]{:S(2)}) copy-start(f32[128]{0:T(128)} %param.13) | copy-start | bytes 1540
  163.2 83.1 %copy-start.5 = (f32[128]{0:T(128)S(1)}, f32[128]{0:T(128)}, u32[]{:S(2)}) copy-start(f32[128]{0:T(128)} %param.12) | copy-start | bytes 1540
Sparse Core Ops, SparseCore 0:
  33.8 91.2 reduce-scatter.2
  127.7 23.4 reduce-scatter.4
  163.3 58.4 all-gather.1
where the time goes:
time: 254 us
  waiting for transfers between devices  176 us (69%)
  blocking collectives  51.4 us (20%)
  between operations  13.2 us (5%)
  matrix products  9.56 us (4%)
  other arithmetic  3.39 us (1%)
    reduce_scatter x2, waiting for transfers between devices, scatter_axes(): nearer = lax.psum_scatter(shard, axes[0], scatter_dimension=dim, tiled=True)  117 us
    all_gather x1, waiting for transfers between devices, whole_of(): shard = lax.all_gather(shard, axis, axis=dim, tiled=True)  58.5 us
    all_to_all x3, blocking collectives, from_everyone(): return lax.all_to_all(copies, axis, split_axis=0, concat_axis=0, tiled=True)  40.4 us
    all_gather x1, blocking collectives, whole_of(): shard = lax.all_gather(shard, axis, axis=dim, tiled=True)  11 us
    dot_general x1, matrix products, per_device(): products = jnp.dot(normed, up_weight, preferred_element_type=jnp.float32)  5.39 us
  transfers between devices with their start and end apart: 3, of which 3 were waited for; matrix products, arithmetic and copies ran while one was open for 0% of the time, Pallas kernels for 0%

commit v1 on v0

v1 whole, which is shorter than its diff:
```python
import functools

import jax
import jax.numpy as jnp
from jax import lax
from jax.experimental import pallas as pl
from jax.experimental.pallas import tpu as pltpu
from jax.sharding import Mesh
from jax.sharding import PartitionSpec as P

CB = ("cb_0", "cb_1")
MESH = pl.DeviceIdType.MESH
NC = 4
ORDER = (0, 2, 1, 3)
EPS = 1e-05
F32 = jnp.float32
BF16 = jnp.bfloat16


def hops(c, di, nz):
    return nz // 2 if (c < NC // 2) == (di == 0) else nz // 2 - 1


def columns_to_rows(a, b):
    n = a.shape[0]
    lane = lax.broadcasted_iota(jnp.int32, (n, 128), 1)
    both = jnp.where(lane == 0, a, jnp.where(lane == 1, b, 0.0))
    return both.T[0:2, :]


def row_to_lanes(row):
    return jnp.broadcast_to(row, (128, row.shape[1])).T


def combine(stats, count):
    sums, squares = stats[:, 0, :], stats[:, 1, :]
    parts = stats.shape[0]
    mean = jnp.sum(sums, axis=0, keepdims=True) / (parts * count)
    apart = sums / count - mean
    total = jnp.sum(squares, axis=0, keepdims=True) + count * jnp.sum(apart * apart, axis=0, keepdims=True)
    return mean, lax.rsqrt(total / (parts * count) + EPS)


def kernel(
    nz, nx, res_hbm, gi_hbm, si_hbm, up_hbm, dn_hbm, go_hbm, so_hbm, out_hbm,
    raw, gi, si, go, so, wup, wdn, st1, normed, rsb, rrb, hid, bacc, xsend, xrecv, sb, rb, st2, outv,
    local_sem, raw_sem, g_sem, up_sem, dn_sem, st1_sem, n_sem, rs_sem, ag_sem, x_sem, br_sem, st2_sem, out_sem,
):
    half = res_hbm.shape[0] // 2
    width = res_hbm.shape[1]
    nq = nz // 2
    h = half // nq
    depth = nx * width
    fc = wdn.shape[0]
    cw = fc // NC
    lm = nz // 2

    r = lax.axis_index("ra")
    z = lax.axis_index("cb_0")
    x = lax.axis_index("cb_1")
    y = lax.axis_index("dp")
    p = lax.rem(y, 2)
    other = 1 - r
    xs = [lax.rem(x + k, nx) for k in range(nx)]
    zs = [lax.rem(z + k, nz) for k in range(nz)]
    ys = [y, y + 1 - 2 * p]
    ps = [p, 1 - p]
    sibling = (other, z, x, y)

    barrier = pltpu.get_barrier_semaphore()
    greeted = [sibling]
    greeted += [(r, z, xs[dx], ys[dj]) for dj in range(2) for dx in range(nx) if dx or dj]
    greeted += [(r, zs[dz], x, y) for dz in range(1, nz)]
    for peer in greeted:
        pl.semaphore_signal(barrier, inc=1, device_id=peer, device_id_type=MESH)

    mine = pl.ds(pl.multiple_of(r * half, half), half)
    own = pl.ds(pl.multiple_of(x * width, width), width)
    first = [
        pltpu.make_async_copy(res_hbm.at[mine, :], raw.at[x, p], local_sem.at[0]),
        pltpu.make_async_copy(gi_hbm, gi.at[x], local_sem.at[1]),
        pltpu.make_async_copy(si_hbm, si.at[x], local_sem.at[2]),
        pltpu.make_async_copy(go_hbm, go, local_sem.at[3]),
        pltpu.make_async_copy(so_hbm, so, local_sem.at[4]),
    ]
    for copy in first:
        copy.start()

    def share(xd):
        return (xd * 2 + p) * fc

    up_own = []
    for c in range(NC):
        cols = pl.ds(pl.multiple_of(share(x) + c * cw, cw), cw)
        up_own.append(pltpu.make_async_copy(up_hbm.at[:, cols], wup.at[c, own, :], local_sem.at[5 + c]))
        up_own[-1].start()
    dn_own = pltpu.make_async_copy(
        dn_hbm.at[pl.ds(pl.multiple_of(share(x), fc), fc), :], wdn.at[:, own], local_sem.at[5 + NC]
    )
    dn_own.start()

    sent = []

    def remote(src, dst, sems, index, peer):
        copy = pltpu.make_async_remote_copy(
            src_ref=src, dst_ref=dst, send_sem=sems.at[(0, *index)], recv_sem=sems.at[(1, *index)],
            device_id=peer, device_id_type=MESH,
        )
        copy.start()
        sent.append(copy)

    def arrived(dst, sems, index):
        pltpu.make_async_remote_copy(
            src_ref=dst, dst_ref=dst, send_sem=sems.at[(0, *index)], recv_sem=sems.at[(1, *index)],
            device_id=sibling, device_id_type=MESH,
        ).wait_recv()

    for copy in first:
        copy.wait()
    pl.semaphore_wait(barrier, len(greeted))

    for dj in range(2):
        for dx in range(nx):
            if dx or dj:
                remote(raw.at[x, p], raw.at[x, p], raw_sem, (dj, dx), (r, z, xs[dx], ys[dj]))
    for dx in range(1, nx):
        peer = (r, z, xs[dx], y)
        remote(gi.at[x], gi.at[x], g_sem, (0, dx), peer)
        remote(si.at[x], si.at[x], g_sem, (1, dx), peer)
    for c in ORDER:
        for dx in range(1, nx):
            cols = pl.ds(pl.multiple_of(share(xs[dx]) + c * cw, cw), cw)
            remote(up_hbm.at[:, cols], wup.at[c, own, :], up_sem, (c, dx), (r, z, xs[dx], y))
    for dx in range(1, nx):
        rows = pl.ds(pl.multiple_of(share(xs[dx]), fc), fc)
        remote(dn_hbm.at[rows, :], wdn.at[:, own], dn_sem, (dx,), (r, z, xs[dx], y))

    for dj in range(2):
        for dx in range(nx):
            if dx or dj:
                arrived(raw.at[xs[nx - dx] if dx else x, ps[dj]], raw_sem, (dj, dx))
    for j in range(2):
        values = [raw[k, j].astype(F32) for k in range(nx)]
        total = jnp.sum(functools.reduce(jnp.add, values), axis=1, keepdims=True)
        mean = total / depth
        apart = [v - mean for v in values]
        square = jnp.sum(functools.reduce(jnp.add, [a * a for a in apart]), axis=1, keepdims=True)
        st1[z, :, j * half : (j + 1) * half] = columns_to_rows(total, square)
    for dz in range(1, nz):
        remote(st1.at[z], st1.at[z], st1_sem, (dz,), (r, zs[dz], x, y))
    for dx in range(1, nx):
        arrived(gi.at[xs[nx - dx]], g_sem, (0, dx))
        arrived(si.at[xs[nx - dx]], g_sem, (1, dx))
    for dz in range(1, nz):
        arrived(st1.at[zs[nz - dz]], st1_sem, (dz,))
    mean, scale = combine(st1[...], depth)
    for j in range(2):
        part = slice(j * half, (j + 1) * half)
        mean_j, scale_j = row_to_lanes(mean[:, part]), row_to_lanes(scale[:, part])
        for k in range(nx):
            v = (raw[k, j].astype(F32) - mean_j) * scale_j * gi[k] + si[k]
            normed[j * nq : (j + 1) * nq, r, :, k * width : (k + 1) * width] = v.astype(BF16).reshape(nq, h, width)
    remote(normed.at[:, r], normed.at[:, r], n_sem, (), sibling)
    arrived(normed.at[:, other], n_sem, ())

    def partial(d, c):
        return jnp.dot(normed[d].reshape(2 * h, depth), wup[c], preferred_element_type=F32)

    ready = set()

    def step_peer(di):
        return (r, zs[1] if di == 0 else zs[nz - 1], x, y)

    for s in range(lm):
        for c in ORDER:
            if c not in ready:
                ready.add(c)
                up_own[c].wait()
                for dx in range(1, nx):
                    arrived(wup.at[c, pl.ds(pl.multiple_of(xs[nx - dx] * width, width), width), :], up_sem, (c, dx))
            for di in range(2):
                length = hops(c, di, nz)
                if s < length:
                    ahead = length - s
                    value = partial(zs[ahead] if di == 0 else zs[nz - ahead], c)
                    if s:
                        arrived(rrb.at[c, di, s - 1], rs_sem, (c, di, s - 1))
                        value = value + rrb[c, di, s - 1].astype(F32)
                    rsb[c, di, s] = value.astype(BF16)
                    remote(rsb.at[c, di, s], rrb.at[c, di, s], rs_sem, (c, di, s), step_peer(di))
    for c in ORDER:
        value = partial(z, c)
        for di in range(2):
            last = hops(c, di, nz) - 1
            arrived(rrb.at[c, di, last], rs_sem, (c, di, last))
            value = value + rrb[c, di, last].astype(F32)
        hid[c, z] = jnp.square(jnp.maximum(value, 0.0)).astype(BF16)
        for di in range(2):
            remote(hid.at[c, z], hid.at[c, z], ag_sem, (c, di, 0), step_peer(di))

    dn_own.wait()
    for dx in range(1, nx):
        arrived(wdn.at[:, pl.ds(pl.multiple_of(xs[nx - dx] * width, width), width)], dn_sem, (dx,))

    def down(k):
        o = zs[k]
        value = jnp.dot(hid[0, o], wdn[0:cw, :], preferred_element_type=F32)
        for c in range(1, NC):
            value += jnp.dot(hid[c, o], wdn[c * cw : (c + 1) * cw, :], preferred_element_type=F32)
        bacc[o] = value.reshape(2, h, depth)
        xsend[o] = bacc[o, other].astype(BF16)
        remote(xsend.at[o], xrecv.at[o], x_sem, (k,), sibling)

    down(0)
    for s in range(1, lm + 1):
        for c in ORDER:
            for di in range(2):
                length = hops(c, di, nz)
                if s <= length:
                    o = zs[nz - s] if di == 0 else zs[s]
                    arrived(hid.at[c, o], ag_sem, (c, di, s - 1))
                    if s < length:
                        remote(hid.at[c, o], hid.at[c, o], ag_sem, (c, di, s), step_peer(di))
        down(s)
        if s < lm:
            down(nz - s)
    for k in range(nz):
        o = zs[k]
        arrived(xrecv.at[o], x_sem, (k,))
        sb[o] = (bacc[o, r] + xrecv[o].astype(F32)).astype(BF16)

    for dj in range(2):
        for dx in range(nx):
            if dx or dj:
                blocks = pl.ds(pl.multiple_of(ps[dj] * nq, nq), nq)
                cols = pl.ds(pl.multiple_of(xs[dx] * width, width), width)
                remote(sb.at[blocks, :, cols], rb.at[dj, dx], br_sem, (dj, dx), (r, z, xs[dx], ys[dj]))
    blocks = pl.ds(pl.multiple_of(p * nq, nq), nq)
    total = 2.0**0.25 * normed[blocks, r, :, own].astype(F32) + sb[blocks, :, own].astype(F32)
    for dj in range(2):
        for dx in range(nx):
            if dx or dj:
                arrived(rb.at[dj, dx], br_sem, (dj, dx))
                total = total + rb[dj, dx].astype(F32)
    total = total.reshape(half, width)
    sums = jnp.sum(total, axis=1, keepdims=True)
    apart = total - sums / width
    st2[0] = columns_to_rows(sums, jnp.sum(apart * apart, axis=1, keepdims=True))
    for k in range(1, nz * nx):
        remote(st2.at[0], st2.at[k], st2_sem, (k,), (r, zs[k // nx], xs[k % nx], y))
    for k in range(1, nz * nx):
        arrived(st2.at[k], st2_sem, (k,))
    mean, scale = combine(st2[...], width)
    outv[...] = ((total - row_to_lanes(mean)) * row_to_lanes(scale) * go[...] + so[...]).astype(BF16)
    keep = pltpu.make_async_copy(outv, out_hbm.at[mine, :], local_sem.at[6 + NC])
    keep.start()
    remote(outv, out_hbm.at[mine, :], out_sem, (), sibling)
    keep.wait()
    arrived(out_hbm.at[pl.ds(pl.multiple_of(other * half, half), half), :], out_sem, ())
    for copy in sent:
        copy.wait_send()


def per_device(nz, nx, residual_in, gain_in, shift_in, up_weight, down_weight, gain_out, shift_out):
    tokens, width = residual_in.shape
    half, nq, depth = tokens // 2, nz // 2, nx * width
    h = half // nq
    fc = up_weight.shape[1] // (2 * nx)
    cw = fc // NC
    dma = pltpu.SemaphoreType.DMA
    row = (1, width)
    return pl.pallas_call(
        functools.partial(kernel, nz, nx),
        out_shape=jax.ShapeDtypeStruct((tokens, width), BF16),
        in_specs=[pl.BlockSpec(memory_space=pl.ANY)] * 7,
        out_specs=pl.BlockSpec(memory_space=pl.ANY),
        scratch_shapes=[
            pltpu.VMEM((nx, 2, half, width), BF16),
            pltpu.VMEM((nx, *row), F32),
            pltpu.VMEM((nx, *row), F32),
            pltpu.VMEM(row, F32),
            pltpu.VMEM(row, F32),
            pltpu.VMEM((NC, depth, cw), BF16),
            pltpu.VMEM((fc, depth), BF16),
            pltpu.VMEM((nz, 2, 2 * half), F32),
            pltpu.VMEM((nz, 2, h, depth), BF16),
            pltpu.VMEM((NC, 2, nq, 2 * h, cw), BF16),
            pltpu.VMEM((NC, 2, nq, 2 * h, cw), BF16),
            pltpu.VMEM((NC, nz, 2 * h, cw), BF16),
            pltpu.VMEM((nz, 2, h, depth), F32),
            pltpu.VMEM((nz, h, depth), BF16),
            pltpu.VMEM((nz, h, depth), BF16),
            pltpu.VMEM((nz, h, depth), BF16),
            pltpu.VMEM((2, nx, nq, h, width), BF16),
            pltpu.VMEM((nz * nx, 2, half), F32),
            pltpu.VMEM((half, width), BF16),
            dma((7 + NC,)),
            dma((2, 2, nx)),
            dma((2, 2, nx)),
            dma((2, NC, nx)),
            dma((2, nx)),
            dma((2, nz)),
            dma((2,)),
            dma((2, NC, 2, nq)),
            dma((2, NC, 2, nq)),
            dma((2, nz)),
            dma((2, 2, nx)),
            dma((2, nz * nx)),
            dma((2,)),
        ],
        compiler_params=pltpu.CompilerParams(collective_id=0, has_side_effects=True),
    )(
        residual_in, gain_in.reshape(row), shift_in.reshape(row), up_weight, down_weight,
        gain_out.reshape(row), shift_out.reshape(row),
    )


def solution(mesh):
    nz, nx = 8, 4
    split = Mesh(
        mesh.devices.reshape(mesh.shape["ra"], nz, nx, mesh.shape["dp"]), ("ra", "cb_0", "cb_1", "dp")
    )
    placed = (P("dp", CB), P(CB), P(CB), P(CB, "ra"), P("ra", CB), P(CB), P(CB))
    return jax.shard_map(
        functools.partial(per_device, nz, nx), mesh=split, in_specs=placed, out_specs=P("dp", CB), check_vma=False
    )
```

time: 254 us -> 75.9 us (0.30)
  waiting for transfers between devices: 176 us -> 0 us
  Pallas kernels: 0 us -> 74.3 us
  blocking collectives: 51.4 us -> 0 us
  between operations: 13.2 us -> 0.01 us
  matrix products: 9.56 us -> 0 us
  other arithmetic: 3.39 us -> 0 us
    reduce_scatter x2 -> x0, waiting for transfers between devices: 117 us -> none  [scatter_axes(): nearer = lax.psum_scatter(shard, axes[0], scatter_dimension=dim, tiled=True)]
    pallas_call x0 -> x1, Pallas kernels: none -> 74.3 us  [per_device(): pl.pallas_call(functools.partial(kernel, nz, nx), out_shape=jax.ShapeDtyp...]
    all_gather x1 -> x0, waiting for transfers between devices: 58.5 us -> none  [whole_of(): shard = lax.all_gather(shard, axis, axis=dim, tiled=True)]
    all_to_all x3 -> x0, blocking collectives: 40.4 us -> none  [from_everyone(): return lax.all_to_all(copies, axis, split_axis=0, concat_axis=0, tiled=True)]
    all_gather x1 -> x0, blocking collectives: 11 us -> none  [whole_of(): shard = lax.all_gather(shard, axis, axis=dim, tiled=True)]
    dot_general x2 -> x0, matrix products: 9.56 us -> none  [the longest x1 5.39 us: per_device(): products = jnp.dot(normed, up_weight, preferred_element_type=jnp.float32)]
  transfers between devices with their start and end apart: 3 -> 0, of which waited for: 3 -> 0; matrix products, arithmetic and copies ran while one was open for 0% -> 0% of each run, Pallas kernels for 0% -> 0%
where the time goes in v1:
time: 75.9 us; the launch traced here: 75.8 us
  Pallas kernels  74.3 us (98%)
  local copies, waits for them, and re-layouts  1.47 us (2%)
    pallas_call x1, Pallas kernels, per_device(): pl.pallas_call(functools.partial(kernel, nz, nx), out_shape=jax.ShapeDtyp...  74.3 us

profile of v1, /device:TPU:1, one launch (start us, length us, event | category | flops | bytes accessed | tf_op | source)
XLA Modules:
  0.0 75.8 jit_solution(8874817597991495102)
XLA Ops:
  0.0 74.3 %shard_map.73 = bf16[256,128]{1,0:T(8,128)(2,1)} custom-call(bf16[256,128]{1,0:T(8,128)(2,1)} %res_hbm.1, f32[1,128]{1,0:T(1,128)} %bitcast.4, f32[1,128]{1,0:T(1,128)} %bitcast.5, bf16[128,8192]{1,0:T(8,128)(2,1)} %up_hbm.1, bf16[8192,128]{1,0:T(8,128)(2,1)} %dn_hbm.1, f32[1,128]{1,0:T(1,128)} %bitcast.6, f32[1,128]{1,0:T(1,128)} %bitcast.7), custom_call_target="tpu_custom_call" | custom-call | tf_op jit(solution)/shard_map/pallas_call | solution.py:272
  74.3 1.5 %copy.9 = bf16[256,128]{1,0:T(8,128)(2,1)} copy(bf16[256,128]{1,0:T(8,128)(2,1)} %shard_map.73) | data formatting | bytes 131072

commit v2 on v1

v2 whole, which is shorter than its diff:
```python
import functools

import jax
import jax.numpy as jnp
from jax import lax
from jax.experimental import pallas as pl
from jax.experimental.pallas import tpu as pltpu
from jax.sharding import Mesh
from jax.sharding import PartitionSpec as P

CB = ("cb_0", "cb_1")
MESH = pl.DeviceIdType.MESH
NC = 4
ORDER = (0, 2, 1, 3)
EPS = 1e-05
F32 = jnp.float32
BF16 = jnp.bfloat16


def hops(c, di, nz):
    return nz // 2 if (c < NC // 2) == (di == 0) else nz // 2 - 1


def columns_to_rows(a, b):
    n = a.shape[0]
    lane = lax.broadcasted_iota(jnp.int32, (n, 128), 1)
    both = jnp.where(lane == 0, a, jnp.where(lane == 1, b, 0.0))
    return both.T[0:2, :]


def row_to_lanes(row):
    return jnp.broadcast_to(row, (128, row.shape[1])).T


def combine(stats, count):
    sums, squares = stats[:, 0, :], stats[:, 1, :]
    parts = stats.shape[0]
    mean = jnp.sum(sums, axis=0, keepdims=True) / (parts * count)
    apart = sums / count - mean
    total = jnp.sum(squares, axis=0, keepdims=True) + count * jnp.sum(apart * apart, axis=0, keepdims=True)
    return mean, lax.rsqrt(total / (parts * count) + EPS)


def kernel(
    nz, nx, res_hbm, gi_hbm, si_hbm, up_hbm, dn_hbm, go_hbm, so_hbm, out_ref,
    raw, gi, si, go, so, wup, wdn, st1, normed, pbuf, rsb, rrb, hid, bacc, xsend, xrecv, sb, rb, st2, tot,
    local_sem, raw_sem, rawf_sem, g_sem, up_sem, upf_sem, dn_sem, st1_sem, rs_sem, ag_sem, x_sem, br_sem, st2_sem, tot_sem,
):
    half = res_hbm.shape[0] // 2
    width = res_hbm.shape[1]
    nq = nz // 2
    h = half // nq
    depth = nx * width
    fc = wdn.shape[0]
    cw = fc // NC
    lm = nz // 2

    r = lax.axis_index("ra")
    z = lax.axis_index("cb_0")
    x = lax.axis_index("cb_1")
    y = lax.axis_index("dp")
    q = lax.rem(y, 2)
    pf = lax.rem(lax.div(y + 1, 2), 2)
    w = lax.div(y, 2)
    yw = 3 - y
    other = 1 - r
    xs = [lax.rem(x + k, nx) for k in range(nx)]
    zs = [lax.rem(z + k, nz) for k in range(nz)]
    ys = [y, y + 1 - 2 * q]
    qs = [q, 1 - q]
    sibling = (other, z, x, y)
    partner = (r, z, x, yw)

    def source(dx):
        return xs[nx - dx] if dx else x

    barrier = pltpu.get_barrier_semaphore()
    greeted = [sibling, partner]
    greeted += [(r, z, xs[dx], ys[dj]) for dj in range(2) for dx in range(nx) if dx or dj]
    greeted += [(c, zs[dz], x, y) for dz in range(1, nz) for c in (r, other)]
    for peer in greeted:
        pl.semaphore_signal(barrier, inc=1, device_id=peer, device_id_type=MESH)

    own = pl.ds(pl.multiple_of(x * width, width), width)
    first = [
        pltpu.make_async_copy(res_hbm.at[0:half, :], raw.at[0, x, q], local_sem.at[0]),
        pltpu.make_async_copy(res_hbm.at[half : 2 * half, :], raw.at[1, x, q], local_sem.at[1]),
        pltpu.make_async_copy(gi_hbm, gi.at[x], local_sem.at[2]),
        pltpu.make_async_copy(si_hbm, si.at[x], local_sem.at[3]),
        pltpu.make_async_copy(go_hbm, go, local_sem.at[4]),
        pltpu.make_async_copy(so_hbm, so, local_sem.at[5]),
    ]
    for copy in first:
        copy.start()

    def share(xd):
        return (xd * 2 + pf) * fc

    up_own = []
    for c in range(NC):
        cols = pl.ds(pl.multiple_of(share(x) + c * cw, cw), cw)
        up_own.append(pltpu.make_async_copy(up_hbm.at[:, cols], wup.at[c, own, :], local_sem.at[6 + c]))
        up_own[-1].start()
    dn_own = pltpu.make_async_copy(
        dn_hbm.at[pl.ds(pl.multiple_of(share(x), fc), fc), :], wdn.at[:, own], local_sem.at[6 + NC]
    )
    dn_own.start()

    sent = []

    def describe(src, dst, sems, index, peer):
        return pltpu.make_async_remote_copy(
            src_ref=src, dst_ref=dst, send_sem=sems.at[(0, *index)], recv_sem=sems.at[(1, *index)],
            device_id=peer, device_id_type=MESH,
        )

    def remote(src, dst, sems, index, peer):
        copy = describe(src, dst, sems, index, peer)
        copy.start()
        sent.append((copy, None))

    def remote_if(condition, src, dst, sems, index, peer):
        copy = describe(src, dst, sems, index, peer)
        pl.when(condition)(copy.start)
        sent.append((copy, condition))

    def arrived(dst, sems, index):
        describe(dst, dst, sems, index, sibling).wait_recv()

    for copy in first:
        copy.wait()
    pl.semaphore_wait(barrier, len(greeted))

    hw = width // 2

    def up_rows(xd, part):
        return pl.ds(pl.multiple_of(xd * width + part * hw, hw), hw)

    for dj in range(2):
        for dx in range(nx):
            if dx or dj:
                remote(raw.at[r, x, q], raw.at[r, x, q], raw_sem, (dj, dx), (r, z, xs[dx], ys[dj]))
    for dx in range(1, nx):
        peer = (r, z, xs[dx], y)
        remote(gi.at[x], gi.at[x], g_sem, (0, dx), peer)
        remote(si.at[x], si.at[x], g_sem, (1, dx), peer)
    for c in ORDER:
        for dx in range(1, nx):
            cols = pl.ds(pl.multiple_of(share(xs[dx]) + c * cw, cw), cw)
            rows = pl.ds(pl.multiple_of(w * hw, hw), hw)
            remote(up_hbm.at[rows, cols], wup.at[c, up_rows(x, w), :], up_sem, (c, dx), (r, z, xs[dx], y))

    def forward_up(c):
        for dx in range(1, nx):
            block = wup.at[c, up_rows(source(dx), w), :]
            arrived(block, up_sem, (c, dx))
            remote(block, block, upf_sem, (c, dx), partner)

    for dj in range(2):
        for dx in range(nx):
            if dx or dj:
                block = raw.at[r, source(dx), qs[dj]]
                arrived(block, raw_sem, (dj, dx))
                remote(block, block, rawf_sem, (dj, dx), sibling)
    for j in range(2):
        values = [raw[r, k, j].astype(F32) for k in range(nx)]
        total = jnp.sum(functools.reduce(jnp.add, values), axis=1, keepdims=True)
        mean = total / depth
        apart = [v - mean for v in values]
        square = jnp.sum(functools.reduce(jnp.add, [a * a for a in apart]), axis=1, keepdims=True)
        st1[r, z, :, j * half : (j + 1) * half] = columns_to_rows(total, square)
    for dz in range(nz):
        for t, core in enumerate((r, other)):
            if dz or t:
                remote(st1.at[r, z], st1.at[r, z], st1_sem, (t, dz), (core, zs[dz], x, y))
    forward_up(ORDER[0])
    for dx in range(1, nx):
        rows = pl.ds(pl.multiple_of(share(xs[dx]), fc), fc)
        remote(dn_hbm.at[rows, :], wdn.at[:, own], dn_sem, (dx,), (r, z, xs[dx], y))
    forward_up(ORDER[1])
    for dx in range(1, nx):
        arrived(gi.at[source(dx)], g_sem, (0, dx))
        arrived(si.at[source(dx)], g_sem, (1, dx))
    for dj in range(2):
        for dx in range(nx):
            if dx or dj:
                arrived(raw.at[other, source(dx), qs[dj]], rawf_sem, (dj, dx))
    for dz in range(nz):
        for t, core in enumerate((r, other)):
            if dz or t:
                arrived(st1.at[core, zs[nz - dz] if dz else z], st1_sem, (t, dz))
    for i in range(2):
        mean, scale = combine(st1[i], depth)
        for j in range(2):
            part = slice(j * half, (j + 1) * half)
            mean_j, scale_j = row_to_lanes(mean[:, part]), row_to_lanes(scale[:, part])
            for k in range(nx):
                v = (raw[i, k, j].astype(F32) - mean_j) * scale_j * gi[k] + si[k]
                normed[j * nq : (j + 1) * nq, i, :, k * width : (k + 1) * width] = v.astype(BF16).reshape(nq, h, width)

    def partials(blocks, c):
        rows = jnp.concatenate([normed[d].reshape(2 * h, depth) for d in blocks], axis=0)
        both = jnp.dot(rows, wup[c], preferred_element_type=F32)
        return [both[i * 2 * h : (i + 1) * 2 * h] for i in range(len(blocks))]

    def active(c, s):
        return [di for di in range(2) if s < hops(c, di, nz)]

    def target(c, di, s):
        ahead = hops(c, di, nz) - s
        return zs[ahead] if di == 0 else zs[nz - ahead]

    def step_peer(di):
        return (r, zs[1] if di == 0 else zs[nz - 1], x, y)

    def pass_on(c, di, s, value):
        rsb[c, di, s] = value.astype(BF16)
        remote(rsb.at[c, di, s], rrb.at[c, di, s], rs_sem, (c, di, s), step_peer(di))

    forward_up(ORDER[2])
    for c in ORDER:
        up_own[c].wait()
        for dx in range(1, nx):
            arrived(wup.at[c, up_rows(source(dx), 1 - w), :], upf_sem, (c, dx))
        for di, value in zip(active(c, 0), partials([target(c, di, 0) for di in active(c, 0)], c)):
            pass_on(c, di, 0, value)
        if c == ORDER[0]:
            forward_up(ORDER[3])
    for s in range(1, lm + 1):
        for c in ORDER:
            if s < lm:
                blocks = [target(c, di, s) for di in active(c, s)]
                if s == lm - 1:
                    blocks.append(z)
                for slot, value in zip(active(c, s) + [2], partials(blocks, c)):
                    pbuf[c, slot] = value
        for c in ORDER:
            if s < lm:
                for di in active(c, s):
                    arrived(rrb.at[c, di, s - 1], rs_sem, (c, di, s - 1))
                    pass_on(c, di, s, pbuf[c, di] + rrb[c, di, s - 1].astype(F32))
            else:
                value = pbuf[c, 2]
                for di in range(2):
                    last = hops(c, di, nz) - 1
                    arrived(rrb.at[c, di, last], rs_sem, (c, di, last))
                    value = value + rrb[c, di, last].astype(F32)
                hid[c, z] = jnp.square(jnp.maximum(value, 0.0)).astype(BF16)
                for di in range(2):
                    remote(hid.at[c, z], hid.at[c, z], ag_sem, (c, di, 0), step_peer(di))

    def down(ks):
        value = 0.0
        for c in range(NC):
            rows = jnp.concatenate([hid[c, zs[k]] for k in ks], axis=0)
            value += jnp.dot(rows, wdn[c * cw : (c + 1) * cw, :], preferred_element_type=F32)
        for i, k in enumerate(ks):
            o = zs[k]
            bacc[o] = value[i * 2 * h : (i + 1) * 2 * h].reshape(2, h, depth)
            xsend[o] = bacc[o, other].astype(BF16)
            remote(xsend.at[o], xrecv.at[o], x_sem, (k,), sibling)

    def branch(ks):
        for k in ks:
            o = zs[k]
            arrived(xrecv.at[o], x_sem, (k,))
            sb[o] = (bacc[o, r] + xrecv[o].astype(F32)).astype(BF16)
            j, i = lax.div(o, nq), lax.rem(o, nq)
            dj = lax.rem(j + q, 2)
            for dx in range(nx):
                cols = pl.ds(pl.multiple_of(xs[dx] * width, width), width)
                args = (sb.at[o, :, cols], rb.at[dj, dx, i], br_sem, (dj, dx, i), (r, z, xs[dx], y - q + j))
                if dx:
                    remote(*args)
                else:
                    remote_if(dj != 0, *args)

    for s in range(1, lm + 1):
        for c in ORDER:
            for di in range(2):
                length = hops(c, di, nz)
                if s <= length:
                    o = zs[nz - s] if di == 0 else zs[s]
                    arrived(hid.at[c, o], ag_sem, (c, di, s - 1))
                    if s < length:
                        remote(hid.at[c, o], hid.at[c, o], ag_sem, (c, di, s), step_peer(di))
        if s == 1:
            dn_own.wait()
            for dx in range(1, nx):
                arrived(wdn.at[:, pl.ds(pl.multiple_of(source(dx) * width, width), width)], dn_sem, (dx,))
            down((0, 1, nz - 1))
        elif s == 2:
            down((2, nz - 2))
            branch((0, 1, nz - 1))
        elif s < lm:
            down((s, nz - s))
            branch((s - 1, nz - s + 1))
        else:
            down((s,))
            branch((s - 1, nz - s + 1))
            branch((s,))

    blocks = pl.ds(pl.multiple_of(q * nq, nq), nq)
    total = 2.0**0.25 * normed[blocks, r, :, own].astype(F32) + sb[blocks, :, own].astype(F32)
    for dj in range(2):
        for dx in range(nx):
            if dx or dj:
                for i in range(nq):
                    arrived(rb.at[dj, dx, i], br_sem, (dj, dx, i))
                total = total + rb[dj, dx].astype(F32)
    total = total.reshape(half, width)
    tot[r] = total
    remote(tot.at[r], tot.at[r], tot_sem, (), sibling)
    sums = jnp.sum(total, axis=1, keepdims=True)
    apart = total - sums / width
    st2[r, 0] = columns_to_rows(sums, jnp.sum(apart * apart, axis=1, keepdims=True))
    for k in range(nz * nx):
        for t, core in enumerate((r, other)):
            if k or t:
                remote(st2.at[r, 0], st2.at[r, k], st2_sem, (t, k), (core, zs[k // nx], xs[k % nx], y))
    arrived(tot.at[other], tot_sem, ())
    for k in range(nz * nx):
        for t, core in enumerate((r, other)):
            if k or t:
                arrived(st2.at[core, k], st2_sem, (t, k))
    for i in range(2):
        mean, scale = combine(st2[i], width)
        out = (tot[i] - row_to_lanes(mean)) * row_to_lanes(scale) * go[...] + so[...]
        out_ref[i * half : (i + 1) * half, :] = out.astype(BF16)
    for copy, condition in sent:
        if condition is None:
            copy.wait_send()
        else:
            pl.when(condition)(copy.wait_send)


def per_device(nz, nx, residual_in, gain_in, shift_in, up_weight, down_weight, gain_out, shift_out):
    tokens, width = residual_in.shape
    half, nq, depth = tokens // 2, nz // 2, nx * width
    h = half // nq
    fc = up_weight.shape[1] // (2 * nx)
    cw = fc // NC
    dma = pltpu.SemaphoreType.DMA
    row = (1, width)
    return pl.pallas_call(
        functools.partial(kernel, nz, nx),
        out_shape=pltpu.VMEM((tokens, width), BF16),
        in_specs=[pl.BlockSpec(memory_space=pl.ANY)] * 7,
        out_specs=pl.BlockSpec(memory_space=pltpu.VMEM),
        scratch_shapes=[
            pltpu.VMEM((2, nx, 2, half, width), BF16),
            pltpu.VMEM((nx, *row), F32),
            pltpu.VMEM((nx, *row), F32),
            pltpu.VMEM(row, F32),
            pltpu.VMEM(row, F32),
            pltpu.VMEM((NC, depth, cw), BF16),
            pltpu.VMEM((fc, depth), BF16),
            pltpu.VMEM((2, nz, 2, 2 * half), F32),
            pltpu.VMEM((nz, 2, h, depth), BF16),
            pltpu.VMEM((NC, 3, 2 * h, cw), F32),
            pltpu.VMEM((NC, 2, nq, 2 * h, cw), BF16),
            pltpu.VMEM((NC, 2, nq, 2 * h, cw), BF16),
            pltpu.VMEM((NC, nz, 2 * h, cw), BF16),
            pltpu.VMEM((nz, 2, h, depth), F32),
            pltpu.VMEM((nz, h, depth), BF16),
            pltpu.VMEM((nz, h, depth), BF16),
            pltpu.VMEM((nz, h, depth), BF16),
            pltpu.VMEM((2, nx, nq, h, width), BF16),
            pltpu.VMEM((2, nz * nx, 2, half), F32),
            pltpu.VMEM((2, half, width), F32),
            dma((7 + NC,)),
            dma((2, 2, nx)),
            dma((2, 2, nx)),
            dma((2, 2, nx)),
            dma((2, NC, nx)),
            dma((2, NC, nx)),
            dma((2, nx)),
            dma((2, 2, nz)),
            dma((2, NC, 2, nq)),
            dma((2, NC, 2, nq)),
            dma((2, nz)),
            dma((2, 2, nx, nq)),
            dma((2, 2, nz * nx)),
            dma((2,)),
        ],
        compiler_params=pltpu.CompilerParams(collective_id=0, has_side_effects=True),
    )(
        residual_in, gain_in.reshape(row), shift_in.reshape(row), up_weight, down_weight,
        gain_out.reshape(row), shift_out.reshape(row),
    )


def solution(mesh):
    nz, nx = 8, 4
    split = Mesh(
        mesh.devices.reshape(mesh.shape["ra"], nz, nx, mesh.shape["dp"]), ("ra", "cb_0", "cb_1", "dp")
    )
    placed = (P("dp", CB), P(CB), P(CB), P(CB, "ra"), P("ra", CB), P(CB), P(CB))
    return jax.shard_map(
        functools.partial(per_device, nz, nx), mesh=split, in_specs=placed, out_specs=P("dp", CB), check_vma=False
    )
```

time: 75.9 us -> 72.1 us (0.950)
  Pallas kernels: 74.3 us -> 71.3 us
  local copies, waits for them, and re-layouts: 1.47 us -> 0.63 us
    pallas_call x1, Pallas kernels: 74.3 us -> 71.3 us  [per_device(): pl.pallas_call(functools.partial(kernel, nz, nx), out_shape=pltpu.VMEM((t...]
    unnamed x1, local copies, waits for them, and re-layouts: 1.47 us -> 0.63 us
where the time goes in v2:
time: 72.1 us; the launch traced here: 72 us
  Pallas kernels  71.3 us (99%)
    pallas_call x1, Pallas kernels, per_device(): pl.pallas_call(functools.partial(kernel, nz, nx), out_shape=pltpu.VMEM((t...  71.3 us

profile of v2, /device:TPU:1, one launch (start us, length us, event | category | flops | bytes accessed | tf_op | source)
XLA Modules:
  0.0 72.0 jit_solution(11336261327537287033)
XLA Ops:
  0.0 71.3 %shard_map.73 = bf16[256,128]{1,0:T(8,128)(2,1)S(1)} custom-call(bf16[256,128]{1,0:T(8,128)(2,1)} %res_hbm.1, f32[1,128]{1,0:T(1,128)} %bitcast.4, f32[1,128]{1,0:T(1,128)} %bitcast.5, bf16[128,8192]{1,0:T(8,128)(2,1)} %up_hbm.1, bf16[8192,128]{1,0:T(8,128)(2,1)} %dn_hbm.1, f32[1,128]{1,0:T(1,128)} %bitcast.6, f32[1,128]{1,0:T(1,128)} %bitcast.7), custom_call_target="tpu_custom_call" | custom-call | tf_op jit(solution)/shard_map/pallas_call | solution.py:345
  71.3 0.6 copy.9

commit v3 on v2

v3 whole, which is shorter than its diff:
```python
import functools

import jax
import jax.numpy as jnp
from jax import lax
from jax.experimental import pallas as pl
from jax.experimental.pallas import tpu as pltpu
from jax.sharding import Mesh
from jax.sharding import PartitionSpec as P

CB = ("cb_0", "cb_1")
MESH = pl.DeviceIdType.MESH
NC = 4
ORDER = (0, 2, 1, 3)
FORWARDED = ORDER[:3]
FAR = (4, 3, 5, 2, 6, 1, 7, 0)
EPS = 1e-05
F32 = jnp.float32
BF16 = jnp.bfloat16


def hops(c, di, nz):
    return nz // 2 if (c < NC // 2) == (di == 0) else nz // 2 - 1


def columns_to_rows(a, b):
    n = a.shape[0]
    lane = lax.broadcasted_iota(jnp.int32, (n, 128), 1)
    both = jnp.where(lane == 0, a, jnp.where(lane == 1, b, 0.0))
    return both.T[0:2, :]


def row_to_lanes(row):
    return jnp.broadcast_to(row, (128, row.shape[1])).T


def combine(stats, count):
    sums, squares = stats[:, 0, :], stats[:, 1, :]
    parts = stats.shape[0]
    mean = jnp.sum(sums, axis=0, keepdims=True) / (parts * count)
    apart = sums / count - mean
    total = jnp.sum(squares, axis=0, keepdims=True) + count * jnp.sum(apart * apart, axis=0, keepdims=True)
    return mean, lax.rsqrt(total / (parts * count) + EPS)


def kernel(
    nz, nx, res_hbm, gi_hbm, si_hbm, up_hbm, dn_hbm, go_hbm, so_hbm, out_ref,
    raw, gi, si, go, so, wup, wdn, st1, normed, pbuf, rsb, rrb, hid, bacc, xsend, xrecv, sb, rb, st2, tot,
    local_sem, send_sem, raw_sem, up_sem, one_sem, ring_sem, x_sem,
):
    half = res_hbm.shape[0] // 2
    width = res_hbm.shape[1]
    nq = nz // 2
    h = half // nq
    depth = nx * width
    fc = wdn.shape[0]
    cw = fc // NC
    lm = nz // 2

    r = lax.axis_index("ra")
    z = lax.axis_index("cb_0")
    x = lax.axis_index("cb_1")
    y = lax.axis_index("dp")
    q = lax.rem(y, 2)
    pf = lax.rem(lax.div(y + 1, 2), 2)
    w = lax.div(y, 2)
    yw = 3 - y
    other = 1 - r
    xs = [lax.rem(x + k, nx) for k in range(nx)]
    zs = [lax.rem(z + k, nz) for k in range(nz)]
    ys = [y, y + 1 - 2 * q]
    qs = [q, 1 - q]
    sibling = (other, z, x, y)
    partner = (r, z, x, yw)

    pairs = [(dj, dx) for dx in (2, 1, 3, 0) for dj in (1, 0) if dx or dj]

    def source(dx):
        return xs[nx - dx] if dx else x

    barrier = pltpu.get_barrier_semaphore()
    greeted = [sibling, partner]
    greeted += [(r, z, xs[dx], ys[dj]) for dj in range(2) for dx in range(nx) if dx or dj]
    greeted += [(c, zs[dz], x, y) for dz in range(1, nz) for c in (r, other)]
    for peer in greeted:
        pl.semaphore_signal(barrier, inc=1, device_id=peer, device_id_type=MESH)

    own = pl.ds(pl.multiple_of(x * width, width), width)
    first = [
        pltpu.make_async_copy(res_hbm.at[0:half, :], raw.at[0, x, q], local_sem.at[0]),
        pltpu.make_async_copy(res_hbm.at[half : 2 * half, :], raw.at[1, x, q], local_sem.at[0]),
        pltpu.make_async_copy(gi_hbm, gi.at[x], local_sem.at[1]),
        pltpu.make_async_copy(si_hbm, si.at[x], local_sem.at[1]),
        pltpu.make_async_copy(go_hbm, go, local_sem.at[1]),
        pltpu.make_async_copy(so_hbm, so, local_sem.at[1]),
    ]
    for copy in first:
        copy.start()

    def share(xd):
        return (xd * 2 + pf) * fc

    for c in range(NC):
        cols = pl.ds(pl.multiple_of(share(x) + c * cw, cw), cw)
        pltpu.make_async_copy(up_hbm.at[:, cols], wup.at[c, own, :], local_sem.at[2]).start()
    rows = pl.ds(pl.multiple_of(share(x), fc), fc)
    pltpu.make_async_copy(dn_hbm.at[rows, :], wdn.at[:, own], local_sem.at[2]).start()

    def remote(src, dst, group, recv, peer):
        copy = pltpu.make_async_remote_copy(
            src_ref=src, dst_ref=dst, send_sem=send_sem.at[group], recv_sem=recv, device_id=peer, device_id_type=MESH
        )
        copy.start()

    def arrived(ref, sem):
        pltpu.make_async_copy(ref, ref, sem).wait()

    arrived(hid.at[0:2], local_sem.at[0])
    arrived(gi, local_sem.at[1])
    pl.semaphore_wait(barrier, len(greeted))

    hw = width // 2

    def up_rows(xd, part):
        return pl.ds(pl.multiple_of(xd * width + part * hw, hw), hw)

    for place, (dj, dx) in enumerate(pairs):
        remote(raw.at[r, x, q], raw.at[r, x, q], 0, raw_sem.at[place], (r, z, xs[dx], ys[dj]))
    for dx in range(1, nx):
        peer = (r, z, xs[dx], y)
        remote(gi.at[x], gi.at[x], 1, one_sem.at[0], peer)
        remote(si.at[x], si.at[x], 1, one_sem.at[1], peer)
    for c in ORDER:
        for dx in range(1, nx):
            cols = pl.ds(pl.multiple_of(share(xs[dx]) + c * cw, cw), cw)
            for part in (w,) if c in FORWARDED else (w, 1 - w):
                rows = pl.ds(pl.multiple_of(part * hw, hw), hw)
                remote(up_hbm.at[rows, cols], wup.at[c, up_rows(x, part), :], 2, up_sem.at[0, c], (r, z, xs[dx], y))

    def forward_up(c):
        arrived(hid.at[0 : nx - 1], up_sem.at[0, c])
        for dx in range(1, nx):
            block = wup.at[c, up_rows(xs[dx], w), :]
            remote(block, block, 3, up_sem.at[1, c], partner)

    for place, (dj, dx) in enumerate(pairs):
        block = raw.at[r, source(dx), qs[dj]]
        arrived(block, raw_sem.at[place])
        remote(block, block, 0, one_sem.at[2], sibling)
    for j in range(2):
        values = [raw[r, k, j].astype(F32) for k in range(nx)]
        total = jnp.sum(functools.reduce(jnp.add, values), axis=1, keepdims=True)
        mean = total / depth
        apart = [v - mean for v in values]
        square = jnp.sum(functools.reduce(jnp.add, [a * a for a in apart]), axis=1, keepdims=True)
        st1[r * nz + z, :, j * half : (j + 1) * half] = columns_to_rows(total, square)
    st1_own = st1.at[r * nz + z]
    for dz in FAR:
        for t, core in enumerate((r, other)):
            if dz or t:
                remote(st1_own, st1_own, 1, one_sem.at[3], (core, zs[dz], x, y))
    forward_up(ORDER[0])
    forward_up(ORDER[1])
    arrived(gi.at[1:nx], one_sem.at[0])
    arrived(si.at[1:nx], one_sem.at[1])
    forward_up(ORDER[2])
    arrived(hid.at[0 : len(pairs)], one_sem.at[2])
    arrived(st1.at[1 : 2 * nz], one_sem.at[3])
    for i in range(2):
        mean, scale = combine(st1[i * nz : (i + 1) * nz], depth)
        for j in range(2):
            part = slice(j * half, (j + 1) * half)
            mean_j, scale_j = row_to_lanes(mean[:, part]), row_to_lanes(scale[:, part])
            for k in range(nx):
                v = (raw[i, k, j].astype(F32) - mean_j) * scale_j * gi[k] + si[k]
                normed[j * nq : (j + 1) * nq, i, :, k * width : (k + 1) * width] = v.astype(BF16).reshape(nq, h, width)

    def partials(blocks, c):
        rows = jnp.concatenate([normed[d].reshape(2 * h, depth) for d in blocks], axis=0)
        both = jnp.dot(rows, wup[c], preferred_element_type=F32)
        return [both[i * 2 * h : (i + 1) * 2 * h] for i in range(len(blocks))]

    def active(c, s):
        return [di for di in range(2) if s < hops(c, di, nz)]

    def target(c, di, s):
        ahead = hops(c, di, nz) - s
        return zs[ahead] if di == 0 else zs[nz - ahead]

    def step_peer(di):
        return (r, zs[1] if di == 0 else zs[nz - 1], x, y)

    def pass_on(c, di, s, value):
        rsb[c, s, di] = value.astype(BF16)
        remote(rsb.at[c, s, di], rrb.at[c, s, di], 4, ring_sem.at[0, c, s], step_peer(di))

    def spread(c, di, s):
        block = hid.at[c * nz + (zs[nz - s if s else 0] if di == 0 else zs[s])]
        remote(block, block, 5, ring_sem.at[1, c, s], step_peer(di))

    arrived(hid.at[0 : 2 * NC + 2 * NC], local_sem.at[2])
    for c in ORDER:
        if c in FORWARDED:
            arrived(hid.at[0 : nx - 1], up_sem.at[1, c])
        else:
            arrived(hid.at[0 : 2 * (nx - 1)], up_sem.at[0, c])
        for di, value in zip(active(c, 0), partials([target(c, di, 0) for di in active(c, 0)], c)):
            pass_on(c, di, 0, value)
    for dx in range(1, nx):
        rows = pl.ds(pl.multiple_of(share(xs[dx]), fc), fc)
        remote(dn_hbm.at[rows, :], wdn.at[:, own], 6, one_sem.at[4], (r, z, xs[dx], y))
    for s in range(1, lm + 1):
        for c in ORDER:
            if s < lm:
                blocks = [target(c, di, s) for di in active(c, s)]
                if s == lm - 1:
                    blocks.append(z)
                for slot, value in zip(active(c, s) + [2], partials(blocks, c)):
                    pbuf[c, slot] = value
        for c in ORDER:
            arrived(rrb.at[c, 0, 0 : len(active(c, s - 1))], ring_sem.at[0, c, s - 1])
            if s < lm:
                for di in active(c, s):
                    pass_on(c, di, s, pbuf[c, di] + rrb[c, s - 1, di].astype(F32))
            else:
                value = pbuf[c, 2]
                for di in range(2):
                    value = value + rrb[c, hops(c, di, nz) - 1, di].astype(F32)
                hid[c * nz + z] = jnp.square(jnp.maximum(value, 0.0)).astype(BF16)
                for di in range(2):
                    spread(c, di, 0)

    def down(ks, stage):
        value = 0.0
        for c in range(NC):
            rows = jnp.concatenate([hid[c * nz + zs[k]] for k in ks], axis=0)
            value += jnp.dot(rows, wdn[c * cw : (c + 1) * cw, :], preferred_element_type=F32)
        for i, k in enumerate(ks):
            o = zs[k]
            bacc[o] = value[i * 2 * h : (i + 1) * 2 * h].reshape(2, h, depth)
            xsend[o] = bacc[o, other].astype(BF16)
            remote(xsend.at[o], xrecv.at[o], 0, x_sem.at[stage], sibling)

    def branch(ks, stage):
        arrived(xrecv.at[0 : len(ks)], x_sem.at[stage])
        for k in ks:
            o = zs[k]
            sb[o] = (bacc[o, r] + xrecv[o].astype(F32)).astype(BF16)
            j, i = lax.div(o, nq), lax.rem(o, nq)
            dj = lax.rem(j + q, 2)
            for dx in range(nx):
                cols = pl.ds(pl.multiple_of(xs[dx] * width, width), width)
                send = functools.partial(
                    remote, sb.at[o, :, cols], rb.at[dj, dx, i], 7, one_sem.at[5], (r, z, xs[dx], y - q + j)
                )
                if dx:
                    send()
                else:
                    pl.when(dj != 0)(send)

    stages = [(0, 1, nz - 1)] + [(k, nz - k) for k in range(2, lm)] + [(lm,)]
    for s in range(1, lm + 1):
        for c in ORDER:
            arrived(hid.at[0 : len(active(c, s - 1))], ring_sem.at[1, c, s - 1])
            for di in active(c, s):
                spread(c, di, s)
        if s == 1:
            arrived(wdn.at[0 : (nx - 1) * fc // nx, :], one_sem.at[4])
        down(stages[s - 1], s - 1)
        if s > 1:
            branch(stages[s - 2], s - 2)
    branch(stages[lm - 1], lm - 1)

    blocks = pl.ds(pl.multiple_of(q * nq, nq), nq)
    total = 2.0**0.25 * normed[blocks, r, :, own].astype(F32) + sb[blocks, :, own].astype(F32)
    arrived(hid.at[0 : len(pairs)], one_sem.at[5])
    for dj, dx in pairs:
        total = total + rb[dj, dx].astype(F32)
    total = total.reshape(half, width)
    tot[r] = total
    remote(tot.at[r], tot.at[r], 0, one_sem.at[6], sibling)
    sums = jnp.sum(total, axis=1, keepdims=True)
    apart = total - sums / width
    st2[r * nz * nx] = columns_to_rows(sums, jnp.sum(apart * apart, axis=1, keepdims=True))
    for dz in FAR:
        for dx in range(nx):
            k = dz * nx + dx
            for t, core in enumerate((r, other)):
                if k or t:
                    remote(st2.at[r * nz * nx], st2.at[r * nz * nx + k], 1, one_sem.at[7], (core, zs[dz], xs[dx], y))
    arrived(tot.at[0], one_sem.at[6])
    arrived(st2.at[1 : 2 * nz * nx], one_sem.at[7])
    for i in range(2):
        mean, scale = combine(st2[i * nz * nx : (i + 1) * nz * nx], width)
        out = (tot[i] - row_to_lanes(mean)) * row_to_lanes(scale) * go[...] + so[...]
        out_ref[i * half : (i + 1) * half, :] = out.astype(BF16)
    for group, units in enumerate((
        2 * len(pairs) + nz + 2, 0, (nx - 1) * (NC + 1), (nx - 1) * (NC - 1), len(pairs) * NC, len(pairs) * NC,
        (nx - 1) * nz, len(pairs),
    )):
        if units:
            arrived(hid.at[0:units], send_sem.at[group])
    arrived(hid.at[0:3], send_sem.at[1])


def per_device(nz, nx, residual_in, gain_in, shift_in, up_weight, down_weight, gain_out, shift_out):
    tokens, width = residual_in.shape
    half, nq, depth = tokens // 2, nz // 2, nx * width
    h = half // nq
    fc = up_weight.shape[1] // (2 * nx)
    cw = fc // NC
    dma = pltpu.SemaphoreType.DMA
    row = (1, width)
    return pl.pallas_call(
        functools.partial(kernel, nz, nx),
        out_shape=pltpu.VMEM((tokens, width), BF16),
        in_specs=[pl.BlockSpec(memory_space=pl.ANY)] * 7,
        out_specs=pl.BlockSpec(memory_space=pltpu.VMEM),
        scratch_shapes=[
            pltpu.VMEM((2, nx, 2, half, width), BF16),
            pltpu.VMEM((nx, *row), F32),
            pltpu.VMEM((nx, *row), F32),
            pltpu.VMEM(row, F32),
            pltpu.VMEM(row, F32),
            pltpu.VMEM((NC, depth, cw), BF16),
            pltpu.VMEM((fc, depth), BF16),
            pltpu.VMEM((2 * nz, 2, 2 * half), F32),
            pltpu.VMEM((nz, 2, h, depth), BF16),
            pltpu.VMEM((NC, 3, 2 * h, cw), F32),
            pltpu.VMEM((NC, nq, 2, 2 * h, cw), BF16),
            pltpu.VMEM((NC, nq, 2, 2 * h, cw), BF16),
            pltpu.VMEM((NC * nz, 2 * h, cw), BF16),
            pltpu.VMEM((nz, 2, h, depth), F32),
            pltpu.VMEM((nz, h, depth), BF16),
            pltpu.VMEM((nz, h, depth), BF16),
            pltpu.VMEM((nz, h, depth), BF16),
            pltpu.VMEM((2, nx, nq, h, width), BF16),
            pltpu.VMEM((2 * nz * nx, 2, half), F32),
            pltpu.VMEM((2, half, width), F32),
            dma((3,)),
            dma((8,)),
            dma((2 * nx - 1,)),
            dma((2, NC)),
            dma((8,)),
            dma((2, NC, nq)),
            dma((nq,)),
        ],
        compiler_params=pltpu.CompilerParams(collective_id=0, has_side_effects=True),
    )(
        residual_in, gain_in.reshape(row), shift_in.reshape(row), up_weight, down_weight,
        gain_out.reshape(row), shift_out.reshape(row),
    )


def solution(mesh):
    nz, nx = 8, 4
    split = Mesh(
        mesh.devices.reshape(mesh.shape["ra"], nz, nx, mesh.shape["dp"]), ("ra", "cb_0", "cb_1", "dp")
    )
    placed = (P("dp", CB), P(CB), P(CB), P(CB, "ra"), P("ra", CB), P(CB), P(CB))
    return jax.shard_map(
        functools.partial(per_device, nz, nx), mesh=split, in_specs=placed, out_specs=P("dp", CB), check_vma=False
    )
```

time: 72.1 us -> 67.2 us (0.932)
  Pallas kernels: 71.3 us -> 66.5 us
    pallas_call x1, Pallas kernels: 71.3 us -> 66.5 us  [per_device(): pl.pallas_call(functools.partial(kernel, nz, nx), out_shape=pltpu.VMEM((t...]
where the time goes in v3:
time: 67.2 us; the launch traced here: 67.1 us
  Pallas kernels  66.5 us (99%)
    pallas_call x1, Pallas kernels, per_device(): pl.pallas_call(functools.partial(kernel, nz, nx), out_shape=pltpu.VMEM((t...  66.5 us

profile of v3, /device:TPU:1, one launch (start us, length us, event | category | flops | bytes accessed | tf_op | source)
XLA Modules:
  0.0 67.1 jit_solution(17174719408731705839)
XLA Ops:
  0.0 66.5 %shard_map.73 = bf16[256,128]{1,0:T(8,128)(2,1)S(1)} custom-call(bf16[256,128]{1,0:T(8,128)(2,1)} %res_hbm.1, f32[1,128]{1,0:T(1,128)} %bitcast.4, f32[1,128]{1,0:T(1,128)} %bitcast.5, bf16[128,8192]{1,0:T(8,128)(2,1)} %up_hbm.1, bf16[8192,128]{1,0:T(8,128)(2,1)} %dn_hbm.1, f32[1,128]{1,0:T(1,128)} %bitcast.6, f32[1,128]{1,0:T(1,128)} %bitcast.7), custom_call_target="tpu_custom_call" | custom-call | tf_op jit(solution)/shard_map/pallas_call | solution.py:314
  66.5 0.6 copy.9

commit v4 on v0

v4 whole, which is shorter than its diff:
```python
import functools

import jax
import jax.numpy as jnp
from jax import lax
from jax.experimental import pallas as pl
from jax.experimental.pallas import tpu as pltpu
from jax.sharding import Mesh
from jax.sharding import PartitionSpec as P

CB = ("cb_0", "cb_1")
MESH = pl.DeviceIdType.MESH
NC = 8
ORDER = (4, 0, 5, 1, 6, 2, 7, 3)
FORWARDED = ORDER[:6]
FAR = (4, 3, 5, 2, 6, 1, 7, 0)
MAIN, HELPER = 1, 0
EPS = 1e-05
F32 = jnp.float32
BF16 = jnp.bfloat16


def hops(c, di, nz):
    return nz // 2 if (c < NC // 2) == (di == 0) else nz // 2 - 1


def columns_to_rows(a, b):
    n = a.shape[0]
    lane = lax.broadcasted_iota(jnp.int32, (n, 128), 1)
    both = jnp.where(lane == 0, a, jnp.where(lane == 1, b, 0.0))
    return both.T[0:2, :]


def row_to_lanes(row):
    return jnp.broadcast_to(row, (128, row.shape[1])).T


def combine(stats, count):
    sums, squares = stats[:, 0, :], stats[:, 1, :]
    parts = stats.shape[0]
    mean = jnp.sum(sums, axis=0, keepdims=True) / (parts * count)
    apart = sums / count - mean
    total = jnp.sum(squares, axis=0, keepdims=True) + count * jnp.sum(apart * apart, axis=0, keepdims=True)
    return mean, lax.rsqrt(total / (parts * count) + EPS)


def kernel(
    nz, nx, res_hbm, gi_hbm, si_hbm, up_hbm, dn_hbm, go_hbm, so_hbm, out_ref,
    raw, gi, si, go, so, wup, wdn, st1, normed, pbuf, rsb, rrb, hid, acc, sb, rb, st2, tot,
    local_sem, send_sem, up_sem, one_sem, ring_sem,
):
    tokens, width = res_hbm.shape
    nq = nz // 2
    rows = tokens // nq
    depth = nx * width
    fc = wdn.shape[0]
    fh = fc // 2
    cw = fc // NC
    lm = nz // 2
    hw = width // 2

    r = lax.axis_index("ra")
    z = lax.axis_index("cb_0")
    x = lax.axis_index("cb_1")
    y = lax.axis_index("dp")
    q = lax.rem(y, 2)
    pf = lax.rem(lax.div(y + 1, 2), 2)
    w = lax.div(y, 2)
    yw = 3 - y
    xs = [lax.rem(x + k, nx) for k in range(nx)]
    zs = [lax.rem(z + k, nz) for k in range(nz)]
    ys = [y, y + 1 - 2 * q]
    qs = [q, 1 - q]
    pairs = [(dj, dx) for dx in (2, 1, 3, 0) for dj in (1, 0) if dx or dj]
    own = pl.ds(pl.multiple_of(x * width, width), width)
    unit = hid.at

    def at(core, dz=0, dx=0):
        return (core, zs[dz], xs[dx], y)

    def enter(peers):
        barrier = pltpu.get_barrier_semaphore()
        for peer in peers:
            pl.semaphore_signal(barrier, inc=1, device_id=peer, device_id_type=MESH)
        return lambda: pl.semaphore_wait(barrier, len(peers))

    def remote(src, dst, group, recv, peer):
        copy = pltpu.make_async_remote_copy(
            src_ref=src, dst_ref=dst, send_sem=send_sem.at[group], recv_sem=recv, device_id=peer, device_id_type=MESH
        )
        copy.start()

    def arrived(ref, sem):
        pltpu.make_async_copy(ref, ref, sem).wait()

    def share(xd):
        return pl.multiple_of((xd * 2 + pf) * fh, fh)

    def up_cols(c, xd):
        return pl.ds(pl.multiple_of(share(xd) + c % (NC // 2) * cw, cw), cw)

    def up_rows(xd, part):
        return pl.ds(pl.multiple_of(xd * width + part * hw, hw), hw)

    def dn_rows(core):
        return pl.ds(core * fh, fh)

    def send_up(core):
        for c in ORDER:
            if c // (NC // 2) == core:
                for dx in (2, 1, 3):
                    if c in FORWARDED:
                        part = pl.ds(pl.multiple_of(w * hw, hw), hw)
                        dst = wup.at[c, up_rows(x, w), :]
                        remote(up_hbm.at[part, up_cols(c, xs[dx])], dst, 2, up_sem.at[0, c], at(HELPER, 0, dx))
                    else:
                        dst = wup.at[c, own, :]
                        remote(up_hbm.at[:, up_cols(c, xs[dx])], dst, 2, up_sem.at[1, c], at(MAIN, 0, dx))
                if core == HELPER:
                    remote(up_hbm.at[:, up_cols(c, x)], wup.at[c, own, :], 2, up_sem.at[1, c], at(MAIN))

    def send_down(core):
        for dx in (2, 1, 3):
            src = dn_hbm.at[pl.ds(share(xs[dx]), fh), :]
            remote(src, wdn.at[dn_rows(core), own], 6, one_sem.at[4], at(MAIN, 0, dx))

    def finish():
        mean, scale = combine(st2[0 : nz * nx], width)
        out = (tot[...] - row_to_lanes(mean)) * row_to_lanes(scale) * go[...] + so[...]
        out_ref[...] = out.astype(BF16)

    def helper():
        greeted = enter([(MAIN, z, x, yw), at(MAIN)] + [at(core, 0, dx) for dx in range(1, nx) for core in (0, 1)])
        pltpu.make_async_copy(go_hbm, go, local_sem.at[1]).start()
        pltpu.make_async_copy(so_hbm, so, local_sem.at[1]).start()
        greeted()
        send_up(HELPER)
        for c in FORWARDED:
            arrived(unit[0 : nx - 1], up_sem.at[0, c])
            for dx in range(1, nx):
                block = wup.at[c, up_rows(xs[dx], w), :]
                remote(block, block, 3, up_sem.at[1, c], (MAIN, z, x, yw))
            for dx in range(1, nx):
                block = wup.at[c, up_rows(xs[dx], w), :]
                remote(block, block, 3, up_sem.at[1, c], at(MAIN))
        send_down(HELPER)
        remote(dn_hbm.at[pl.ds(share(x), fh), :], wdn.at[dn_rows(HELPER), own], 6, one_sem.at[4], at(MAIN))
        arrived(gi.at[0:2], local_sem.at[1])
        arrived(unit[0 : (nx - 1) * (NC // 2 + 1) + NC], send_sem.at[2])
        arrived(unit[0 : 2 * (nx - 1) * len(FORWARDED)], send_sem.at[3])
        arrived(unit[0 : nx * NC], send_sem.at[6])
        arrived(unit[0:4], one_sem.at[6])
        arrived(st2.at[0 : nz * nx], one_sem.at[7])
        finish()

    def main():
        greeted = enter(
            [(MAIN, z, xs[dx], ys[dj]) for dj, dx in pairs] + [at(MAIN, dz) for dz in range(1, nz)]
            + [at(HELPER, 0, dx) for dx in range(nx)] + [(HELPER, z, x, yw)]
        )
        pltpu.make_async_copy(res_hbm, raw.at[x, q], local_sem.at[0]).start()
        for src, dst in ((gi_hbm, gi.at[x]), (si_hbm, si.at[x]), (go_hbm, go), (so_hbm, so)):
            pltpu.make_async_copy(src, dst, local_sem.at[1]).start()
        for c in range(NC // 2, NC):
            pltpu.make_async_copy(up_hbm.at[:, up_cols(c, x)], wup.at[c, own, :], local_sem.at[2]).start()
        src = dn_hbm.at[pl.ds(share(x), fh), :]
        pltpu.make_async_copy(src, wdn.at[dn_rows(MAIN), own], local_sem.at[2]).start()
        arrived(unit[0:2], local_sem.at[0])
        arrived(gi, local_sem.at[1])
        greeted()

        for dj, dx in pairs:
            remote(raw.at[x, q], raw.at[x, q], 0, one_sem.at[2 + dj], (MAIN, z, xs[dx], ys[dj]))
        for dx in range(1, nx):
            remote(gi.at[x], gi.at[x], 1, one_sem.at[0], at(MAIN, 0, dx))
            remote(si.at[x], si.at[x], 8, one_sem.at[1], at(MAIN, 0, dx))
        send_up(MAIN)

        for dj in range(2):
            arrived(unit[0 : 2 * (nx - 1 + dj)], one_sem.at[2 + dj])
            values = [raw[k, qs[dj]].astype(F32) for k in range(nx)]
            total = jnp.sum(functools.reduce(jnp.add, values), axis=1, keepdims=True)
            mean = total / depth
            apart = [v - mean for v in values]
            square = jnp.sum(functools.reduce(jnp.add, [a * a for a in apart]), axis=1, keepdims=True)
            st1[z, qs[dj]] = columns_to_rows(total, square)
        for dz in FAR[:-1]:
            remote(st1.at[z], st1.at[z], 9, one_sem.at[8], at(MAIN, dz))
        arrived(gi.at[1:nx], one_sem.at[0])
        arrived(si.at[1:nx], one_sem.at[1])
        arrived(st1.at[1:nz], one_sem.at[8])
        for j in range(2):
            mean, scale = combine(st1[:, j], depth)
            mean, scale = row_to_lanes(mean), row_to_lanes(scale)
            for k in range(nx):
                v = (raw[k, j].astype(F32) - mean) * scale * gi[k] + si[k]
                normed[j * nq : (j + 1) * nq, :, k * width : (k + 1) * width] = v.astype(BF16).reshape(nq, rows, width)

        def partials(blocks, c):
            left = jnp.concatenate([normed[d] for d in blocks], axis=0)
            both = jnp.dot(left, wup[c], preferred_element_type=F32)
            return [both[i * rows : (i + 1) * rows] for i in range(len(blocks))]

        def active(c, s):
            return [di for di in range(2) if s < hops(c, di, nz)]

        def target(c, di, s):
            ahead = hops(c, di, nz) - s
            return zs[ahead] if di == 0 else zs[nz - ahead]

        def pass_on(c, di, s, value):
            rsb[c, s, di] = value.astype(BF16)
            remote(rsb.at[c, s, di], rrb.at[c, s, di], 4, ring_sem.at[0, c, s], at(MAIN, 1 if di == 0 else nz - 1))

        def spread(c, di, s):
            block = unit[c * nz + (zs[nz - s if s else 0] if di == 0 else zs[s])]
            remote(block, block, 5, ring_sem.at[1, c, s], at(MAIN, 1 if di == 0 else nz - 1))

        def prepare(c, s):
            blocks = [target(c, di, s) for di in active(c, s)]
            if s == lm - 1:
                blocks.append(z)
            for slot, value in zip(active(c, s) + [2], partials(blocks, c)):
                pbuf[c, slot] = value

        arrived(unit[0 : 2 * NC], local_sem.at[2])
        for c in ORDER:
            arrived(unit[0 : 2 * (nx - 1) + (2 if c < NC // 2 else 0)], up_sem.at[1, c])
            for di, value in zip(active(c, 0), partials([target(c, di, 0) for di in active(c, 0)], c)):
                pass_on(c, di, 0, value)
            prepare(c, 1)
        send_down(MAIN)
        for s in range(1, lm + 1):
            for c in ORDER:
                arrived(rrb.at[c, 0, 0 : len(active(c, s - 1))], ring_sem.at[0, c, s - 1])
                if s < lm:
                    for di in active(c, s):
                        pass_on(c, di, s, pbuf[c, di] + rrb[c, s - 1, di].astype(F32))
                    if s < lm - 1:
                        prepare(c, s + 1)
                else:
                    value = pbuf[c, 2]
                    for di in range(2):
                        value = value + rrb[c, hops(c, di, nz) - 1, di].astype(F32)
                    hid[c * nz + z] = jnp.square(jnp.maximum(value, 0.0)).astype(BF16)
                    for di in range(2):
                        spread(c, di, 0)

        def down(c, ks):
            left = jnp.concatenate([hid[c * nz + zs[k]] for k in ks], axis=0)
            value = jnp.dot(left, wdn[c * cw : (c + 1) * cw, :], preferred_element_type=F32)
            for i, k in enumerate(ks):
                part = value[i * rows : (i + 1) * rows]
                acc[k] = part if c == ORDER[0] else acc[k] + part

        def branch(ks):
            for k in ks:
                o = zs[k]
                sb[o] = acc[k].astype(BF16)
                j, i = lax.div(o, nq), lax.rem(o, nq)
                dj = lax.rem(j + q, 2)
                for dx in (2, 1, 3, 0):
                    cols = pl.ds(pl.multiple_of(xs[dx] * width, width), width)
                    send = functools.partial(
                        remote, sb.at[o, :, cols], rb.at[dj, dx, i], 7, one_sem.at[5], (MAIN, z, xs[dx], y - q + j)
                    )
                    if dx:
                        send()
                    else:
                        pl.when(dj != 0)(send)

        stages = [(0, 1, nz - 1)] + [(k, nz - k) for k in range(2, lm)] + [(lm,)]
        for s in range(1, lm + 1):
            if s == 2:
                arrived(unit[0 : NC * (nx - 1) * 2 + NC], one_sem.at[4])
            for c in ORDER:
                arrived(unit[0 : len(active(c, s - 1))], ring_sem.at[1, c, s - 1])
                for di in active(c, s):
                    spread(c, di, s)
                if s > 1:
                    down(c, stages[s - 2] if s < lm else stages[s - 1])
            if 1 < s < lm:
                branch(stages[s - 2])
            if s == lm - 1:
                for c in ORDER:
                    down(c, stages[s - 1])
                branch(stages[s - 1])
        branch(stages[lm - 1])

        blocks = pl.ds(pl.multiple_of(q * nq, nq), nq)
        total = 2.0**0.25 * normed[blocks, :, own].astype(F32) + sb[blocks, :, own].astype(F32)
        arrived(unit[0 : 2 * len(pairs)], one_sem.at[5])
        for dj, dx in pairs:
            total = total + rb[dj, dx].astype(F32)
        total = total.reshape(tokens, width)
        sums = jnp.sum(total, axis=1, keepdims=True)
        apart = total - sums / width
        st2[0] = columns_to_rows(sums, jnp.sum(apart * apart, axis=1, keepdims=True))
        tot[...] = total
        for core in (MAIN, HELPER):
            for dz in FAR:
                for dx in (2, 1, 3, 0):
                    k = dz * nx + dx
                    if k or core == HELPER:
                        remote(st2.at[0], st2.at[k], 10, one_sem.at[7], at(core, dz, dx))
            if core == MAIN:
                remote(tot, tot, 0, one_sem.at[6], at(HELPER))
        arrived(st2.at[1 : nz * nx], one_sem.at[7])
        finish()

        for group, ref in (
            (0, unit[0 : 2 * len(pairs) + 4]),
            (1, gi.at[1:nx]),
            (8, si.at[1:nx]),
            (2, unit[0 : (nx - 1) * (NC // 2 + 1)]),
            (4, unit[0 : len(pairs) * NC]),
            (5, unit[0 : len(pairs) * NC]),
            (6, unit[0 : (nx - 1) * NC]),
            (7, unit[0 : 2 * len(pairs)]),
            (9, st1.at[1:nz]),
            (10, st2.at[1 : 2 * nz * nx]),
        ):
            arrived(ref, send_sem.at[group])

    pl.when(r == MAIN)(main)
    pl.when(r == HELPER)(helper)


def per_device(nz, nx, residual_in, gain_in, shift_in, up_weight, down_weight, gain_out, shift_out):
    tokens, width = residual_in.shape
    nq, depth = nz // 2, nx * width
    rows = tokens // nq
    fc = up_weight.shape[1] // nx
    cw = fc // NC
    dma = pltpu.SemaphoreType.DMA
    row = (1, width)
    return pl.pallas_call(
        functools.partial(kernel, nz, nx),
        out_shape=pltpu.VMEM((tokens, width), BF16),
        in_specs=[pl.BlockSpec(memory_space=pl.ANY)] * 7,
        out_specs=pl.BlockSpec(memory_space=pltpu.VMEM),
        scratch_shapes=[
            pltpu.VMEM((nx, 2, tokens, width), BF16),
            pltpu.VMEM((nx, *row), F32),
            pltpu.VMEM((nx, *row), F32),
            pltpu.VMEM(row, F32),
            pltpu.VMEM(row, F32),
            pltpu.VMEM((NC, depth, cw), BF16),
            pltpu.VMEM((fc, depth), BF16),
            pltpu.VMEM((nz, 2, 2, tokens), F32),
            pltpu.VMEM((nz, rows, depth), BF16),
            pltpu.VMEM((NC, 3, rows, cw), F32),
            pltpu.VMEM((NC, nq, 2, rows, cw), BF16),
            pltpu.VMEM((NC, nq, 2, rows, cw), BF16),
            pltpu.VMEM((NC * nz, rows, cw), BF16),
            pltpu.VMEM((nz, rows, depth), F32),
            pltpu.VMEM((nz, rows, depth), BF16),
            pltpu.VMEM((2, nx, nq, rows, width), BF16),
            pltpu.VMEM((2 * nz * nx, 2, tokens), F32),
            pltpu.VMEM((tokens, width), F32),
            dma((3,)),
            dma((11,)),
            dma((2, NC)),
            dma((9,)),
            dma((2, NC, nq)),
        ],
        compiler_params=pltpu.CompilerParams(collective_id=0, has_side_effects=True),
    )(
        residual_in, gain_in.reshape(row), shift_in.reshape(row), up_weight, down_weight,
        gain_out.reshape(row), shift_out.reshape(row),
    )


def solution(mesh):
    nz, nx = 8, 4
    split = Mesh(
        mesh.devices.reshape(mesh.shape["ra"], nz, nx, mesh.shape["dp"]), ("ra", "cb_0", "cb_1", "dp")
    )
    placed = (P("dp", CB), P(CB), P(CB), P(CB, "ra"), P("ra", CB), P(CB), P(CB))
    return jax.shard_map(
        functools.partial(per_device, nz, nx), mesh=split, in_specs=placed, out_specs=P("dp", CB), check_vma=False
    )
```

time: 254 us -> 61.5 us (0.24)
  waiting for transfers between devices: 176 us -> 0 us
  Pallas kernels: 0 us -> 60.7 us
  blocking collectives: 51.4 us -> 0 us
  between operations: 13.2 us -> 0.01 us
  matrix products: 9.56 us -> 0 us
  other arithmetic: 3.39 us -> 0 us
    reduce_scatter x2 -> x0, waiting for transfers between devices: 117 us -> none  [scatter_axes(): nearer = lax.psum_scatter(shard, axes[0], scatter_dimension=dim, tiled=True)]
    pallas_call x0 -> x1, Pallas kernels: none -> 60.7 us  [per_device(): pl.pallas_call(functools.partial(kernel, nz, nx), out_shape=pltpu.VMEM((t...]
    all_gather x1 -> x0, waiting for transfers between devices: 58.5 us -> none  [whole_of(): shard = lax.all_gather(shard, axis, axis=dim, tiled=True)]
    all_to_all x3 -> x0, blocking collectives: 40.4 us -> none  [from_everyone(): return lax.all_to_all(copies, axis, split_axis=0, concat_axis=0, tiled=True)]
    all_gather x1 -> x0, blocking collectives: 11 us -> none  [whole_of(): shard = lax.all_gather(shard, axis, axis=dim, tiled=True)]
    dot_general x2 -> x0, matrix products: 9.56 us -> none  [the longest x1 5.39 us: per_device(): products = jnp.dot(normed, up_weight, preferred_element_type=jnp.float32)]
  transfers between devices with their start and end apart: 3 -> 0, of which waited for: 3 -> 0; matrix products, arithmetic and copies ran while one was open for 0% -> 0% of each run, Pallas kernels for 0% -> 0%
where the time goes in v4:
time: 61.5 us; the launch traced here: 61.4 us
  Pallas kernels  60.7 us (99%)
  local copies, waits for them, and re-layouts  0.63 us (1%)
    pallas_call x1, Pallas kernels, per_device(): pl.pallas_call(functools.partial(kernel, nz, nx), out_shape=pltpu.VMEM((t...  60.7 us

profile of v4, /device:TPU:1, one launch (start us, length us, event | category | flops | bytes accessed | tf_op | source)
XLA Modules:
  0.0 61.4 jit_solution(1229417882835503365)
XLA Ops:
  0.0 60.7 %shard_map.73 = bf16[256,128]{1,0:T(8,128)(2,1)S(1)} custom-call(bf16[256,128]{1,0:T(8,128)(2,1)} %res_hbm.1, f32[1,128]{1,0:T(1,128)} %bitcast.4, f32[1,128]{1,0:T(1,128)} %bitcast.5, bf16[128,8192]{1,0:T(8,128)(2,1)} %up_hbm.1, bf16[8192,128]{1,0:T(8,128)(2,1)} %dn_hbm.1, f32[1,128]{1,0:T(1,128)} %bitcast.6, f32[1,128]{1,0:T(1,128)} %bitcast.7), custom_call_target="tpu_custom_call" | custom-call | tf_op jit(solution)/shard_map/pallas_call | solution.py:337
  60.7 0.6 %copy.9 = bf16[256,128]{1,0:T(8,128)(2,1)} copy(bf16[256,128]{1,0:T(8,128)(2,1)S(1)} %shard_map.73) | data formatting | bytes 131072

commit v5 on v4

--- a/solution.py
+++ b/solution.py
@@ -11,8 +11,8 @@
 CB = ("cb_0", "cb_1")
 MESH = pl.DeviceIdType.MESH
 NC = 8
-ORDER = (4, 0, 5, 1, 6, 2, 7, 3)
-FORWARDED = ORDER[:6]
+ORDER = (0, 1, 2, 3, 4, 5, 6, 7)
+FORWARDED = (0, 1, 2, 4, 5)
 FAR = (4, 3, 5, 2, 6, 1, 7, 0)
 MAIN, HELPER = 1, 0
 EPS = 1e-05
@@ -21,7 +21,7 @@
 
 
 def hops(c, di, nz):
-    return nz // 2 if (c < NC // 2) == (di == 0) else nz // 2 - 1
+    return nz // 2 - (ORDER.index(c) + di) % 2
 
 
 def columns_to_rows(a, b):
@@ -47,7 +47,7 @@
 def kernel(
     nz, nx, res_hbm, gi_hbm, si_hbm, up_hbm, dn_hbm, go_hbm, so_hbm, out_ref,
     raw, gi, si, go, so, wup, wdn, st1, normed, pbuf, rsb, rrb, hid, acc, sb, rb, st2, tot,
-    local_sem, send_sem, up_sem, one_sem, ring_sem,
+    local_sem, send_sem, up_sem, one_sem, ring_sem, reach_sem,
 ):
     tokens, width = res_hbm.shape
     nq = nz // 2
@@ -105,8 +105,8 @@
     def dn_rows(core):
         return pl.ds(core * fh, fh)
 
-    def send_up(core):
-        for c in ORDER:
+    def send_up(core, chunks):
+        for c in chunks:
             if c // (NC // 2) == core:
                 for dx in (2, 1, 3):
                     if c in FORWARDED:
@@ -119,6 +119,9 @@
                 if core == HELPER:
                     remote(up_hbm.at[:, up_cols(c, x)], wup.at[c, own, :], 2, up_sem.at[1, c], at(MAIN))
 
+    def up_units(core):
+        return sum((nx - 1) * (1 if c in FORWARDED else 2) for c in ORDER if c // (NC // 2) == core)
+
     def send_down(core):
         for dx in (2, 1, 3):
             src = dn_hbm.at[pl.ds(share(xs[dx]), fh), :]
@@ -134,7 +137,7 @@
         pltpu.make_async_copy(go_hbm, go, local_sem.at[1]).start()
         pltpu.make_async_copy(so_hbm, so, local_sem.at[1]).start()
         greeted()
-        send_up(HELPER)
+        send_up(HELPER, FORWARDED)
         for c in FORWARDED:
             arrived(unit[0 : nx - 1], up_sem.at[0, c])
             for dx in range(1, nx):
@@ -143,10 +146,12 @@
             for dx in range(1, nx):
                 block = wup.at[c, up_rows(xs[dx], w), :]
                 remote(block, block, 3, up_sem.at[1, c], at(MAIN))
+            if c == FORWARDED[1]:
+                send_up(HELPER, [c for c in ORDER if c not in FORWARDED])
         send_down(HELPER)
         remote(dn_hbm.at[pl.ds(share(x), fh), :], wdn.at[dn_rows(HELPER), own], 6, one_sem.at[4], at(MAIN))
         arrived(gi.at[0:2], local_sem.at[1])
-        arrived(unit[0 : (nx - 1) * (NC // 2 + 1) + NC], send_sem.at[2])
+        arrived(unit[0 : up_units(HELPER) + NC], send_sem.at[2])
         arrived(unit[0 : 2 * (nx - 1) * len(FORWARDED)], send_sem.at[3])
         arrived(unit[0 : nx * NC], send_sem.at[6])
         arrived(unit[0:4], one_sem.at[6])
@@ -155,7 +160,7 @@
 
     def main():
         greeted = enter(
-            [(MAIN, z, xs[dx], ys[dj]) for dj, dx in pairs] + [at(MAIN, dz) for dz in range(1, nz)]
+            [(MAIN, z, xs[dx], ys[dj]) for dj, dx in pairs] + [at(MAIN, dz) for dz in (1, nz - 1)]
             + [at(HELPER, 0, dx) for dx in range(nx)] + [(HELPER, z, x, yw)]
         )
         pltpu.make_async_copy(res_hbm, raw.at[x, q], local_sem.at[0]).start()
@@ -174,7 +179,12 @@
         for dx in range(1, nx):
             remote(gi.at[x], gi.at[x], 1, one_sem.at[0], at(MAIN, 0, dx))
             remote(si.at[x], si.at[x], 8, one_sem.at[1], at(MAIN, 0, dx))
-        send_up(MAIN)
+        send_up(MAIN, ORDER)
+
+        for k in range(lm - 1):
+            for dz in (1, nz - 1):
+                pl.semaphore_signal(reach_sem.at[k], inc=1, device_id=at(MAIN, dz), device_id_type=MESH)
+            pl.semaphore_wait(reach_sem.at[k], 2)
 
         for dj in range(2):
             arrived(unit[0 : 2 * (nx - 1 + dj)], one_sem.at[2 + dj])
@@ -312,7 +322,7 @@
             (0, unit[0 : 2 * len(pairs) + 4]),
             (1, gi.at[1:nx]),
             (8, si.at[1:nx]),
-            (2, unit[0 : (nx - 1) * (NC // 2 + 1)]),
+            (2, unit[0 : up_units(MAIN)]),
             (4, unit[0 : len(pairs) * NC]),
             (5, unit[0 : len(pairs) * NC]),
             (6, unit[0 : (nx - 1) * NC]),
@@ -363,6 +373,7 @@
             dma((2, NC)),
             dma((9,)),
             dma((2, NC, nq)),
+            pltpu.SemaphoreType.REGULAR((nq - 1,)),
         ],
         compiler_params=pltpu.CompilerParams(collective_id=0, has_side_effects=True),
     )(

time: 61.5 us -> 57.4 us (0.933)
  Pallas kernels: 60.7 us -> 56.6 us
    pallas_call x1, Pallas kernels: 60.7 us -> 56.6 us  [per_device(): pl.pallas_call(functools.partial(kernel, nz, nx), out_shape=pltpu.VMEM((t...]
where the time goes in v5:
time: 57.4 us; the launch traced here: 57.3 us
  Pallas kernels  56.6 us (99%)
  local copies, waits for them, and re-layouts  0.63 us (1%)
    pallas_call x1, Pallas kernels, per_device(): pl.pallas_call(functools.partial(kernel, nz, nx), out_shape=pltpu.VMEM((t...  56.6 us

profile of v5, /device:TPU:1, one launch (start us, length us, event | category | flops | bytes accessed | tf_op | source)
XLA Modules:
  0.0 57.3 jit_solution(4122950348064436578)
XLA Ops:
  0.0 56.6 %shard_map.73 = bf16[256,128]{1,0:T(8,128)(2,1)S(1)} custom-call(bf16[256,128]{1,0:T(8,128)(2,1)} %res_hbm.1, f32[1,128]{1,0:T(1,128)} %bitcast.4, f32[1,128]{1,0:T(1,128)} %bitcast.5, bf16[128,8192]{1,0:T(8,128)(2,1)} %up_hbm.1, bf16[8192,128]{1,0:T(8,128)(2,1)} %dn_hbm.1, f32[1,128]{1,0:T(1,128)} %bitcast.6, f32[1,128]{1,0:T(1,128)} %bitcast.7), custom_call_target="tpu_custom_call" | custom-call | tf_op jit(solution)/shard_map/pallas_call | solution.py:347
  56.6 0.6 %copy.9 = bf16[256,128]{1,0:T(8,128)(2,1)} copy(bf16[256,128]{1,0:T(8,128)(2,1)S(1)} %shard_map.73) | data formatting | bytes 131072

commit v6 on v5

--- a/solution.py
+++ b/solution.py
@@ -12,7 +12,8 @@
 MESH = pl.DeviceIdType.MESH
 NC = 8
 ORDER = (0, 1, 2, 3, 4, 5, 6, 7)
-FORWARDED = (0, 1, 2, 4, 5)
+FORWARDED = (0, 1, 2, 4)
+EARLY = (0, 1, 2)
 FAR = (4, 3, 5, 2, 6, 1, 7, 0)
 MAIN, HELPER = 1, 0
 EPS = 1e-05
@@ -35,18 +36,28 @@
     return jnp.broadcast_to(row, (128, row.shape[1])).T
 
 
+def pool(stats, count):
+    sums, squares = stats[:, 0, :], stats[:, 1, :]
+    total = jnp.sum(sums, axis=0, keepdims=True)
+    apart = sums / count - total / (stats.shape[0] * count)
+    return total, jnp.sum(squares, axis=0, keepdims=True) + count * jnp.sum(apart * apart, axis=0, keepdims=True)
+
+
 def combine(stats, count):
-    sums, squares = stats[:, 0, :], stats[:, 1, :]
-    parts = stats.shape[0]
-    mean = jnp.sum(sums, axis=0, keepdims=True) / (parts * count)
-    apart = sums / count - mean
-    total = jnp.sum(squares, axis=0, keepdims=True) + count * jnp.sum(apart * apart, axis=0, keepdims=True)
-    return mean, lax.rsqrt(total / (parts * count) + EPS)
+    total, square = pool(stats, count)
+    whole = stats.shape[0] * count
+    return total / whole, lax.rsqrt(square / whole + EPS)
+
+
+def of_shard(values):
+    sums = jnp.sum(values, axis=1, keepdims=True)
+    apart = values - sums / values.shape[1]
+    return columns_to_rows(sums, jnp.sum(apart * apart, axis=1, keepdims=True))
 
 
 def kernel(
     nz, nx, res_hbm, gi_hbm, si_hbm, up_hbm, dn_hbm, go_hbm, so_hbm, out_ref,
-    raw, gi, si, go, so, wup, wdn, st1, normed, pbuf, rsb, rrb, hid, acc, sb, rb, st2, tot,
+    raw, gi, si, go, so, wup, wdn, st0, st1, normed, pbuf, rsb, rrb, hid, acc, sb, rb, st2, tot,
     local_sem, send_sem, up_sem, one_sem, ring_sem, reach_sem,
 ):
     tokens, width = res_hbm.shape
@@ -137,7 +148,7 @@
         pltpu.make_async_copy(go_hbm, go, local_sem.at[1]).start()
         pltpu.make_async_copy(so_hbm, so, local_sem.at[1]).start()
         greeted()
-        send_up(HELPER, FORWARDED)
+        send_up(HELPER, EARLY)
         for c in FORWARDED:
             arrived(unit[0 : nx - 1], up_sem.at[0, c])
             for dx in range(1, nx):
@@ -146,8 +157,9 @@
             for dx in range(1, nx):
                 block = wup.at[c, up_rows(xs[dx], w), :]
                 remote(block, block, 3, up_sem.at[1, c], at(MAIN))
-            if c == FORWARDED[1]:
-                send_up(HELPER, [c for c in ORDER if c not in FORWARDED])
+            if c == FORWARDED[0]:
+                send_up(HELPER, [c for c in ORDER if c not in EARLY])
+        pl.semaphore_wait(reach_sem.at[lm - 1], 1)
         send_down(HELPER)
         remote(dn_hbm.at[pl.ds(share(x), fh), :], wdn.at[dn_rows(HELPER), own], 6, one_sem.at[4], at(MAIN))
         arrived(gi.at[0:2], local_sem.at[1])
@@ -172,8 +184,11 @@
         pltpu.make_async_copy(src, wdn.at[dn_rows(MAIN), own], local_sem.at[2]).start()
         arrived(unit[0:2], local_sem.at[0])
         arrived(gi, local_sem.at[1])
+        st0[0] = of_shard(raw[x, q].astype(F32))
         greeted()
 
+        for dj, dx in pairs:
+            remote(st0.at[0], st0.at[dj * nx + dx], 11, one_sem.at[9], (MAIN, z, xs[dx], ys[dj]))
         for dj, dx in pairs:
             remote(raw.at[x, q], raw.at[x, q], 0, one_sem.at[2 + dj], (MAIN, z, xs[dx], ys[dj]))
         for dx in range(1, nx):
@@ -186,18 +201,15 @@
                 pl.semaphore_signal(reach_sem.at[k], inc=1, device_id=at(MAIN, dz), device_id_type=MESH)
             pl.semaphore_wait(reach_sem.at[k], 2)
 
+        arrived(st0.at[1 : 2 * nx], one_sem.at[9])
         for dj in range(2):
-            arrived(unit[0 : 2 * (nx - 1 + dj)], one_sem.at[2 + dj])
-            values = [raw[k, qs[dj]].astype(F32) for k in range(nx)]
-            total = jnp.sum(functools.reduce(jnp.add, values), axis=1, keepdims=True)
-            mean = total / depth
-            apart = [v - mean for v in values]
-            square = jnp.sum(functools.reduce(jnp.add, [a * a for a in apart]), axis=1, keepdims=True)
-            st1[z, qs[dj]] = columns_to_rows(total, square)
+            st1[z, qs[dj]] = jnp.concatenate(pool(st0[dj * nx : (dj + 1) * nx], width), axis=0)
         for dz in FAR[:-1]:
             remote(st1.at[z], st1.at[z], 9, one_sem.at[8], at(MAIN, dz))
         arrived(gi.at[1:nx], one_sem.at[0])
         arrived(si.at[1:nx], one_sem.at[1])
+        for dj in range(2):
+            arrived(unit[0 : 2 * (nx - 1 + dj)], one_sem.at[2 + dj])
         arrived(st1.at[1:nz], one_sem.at[8])
         for j in range(2):
             mean, scale = combine(st1[:, j], depth)
@@ -220,11 +232,11 @@
 
         def pass_on(c, di, s, value):
             rsb[c, s, di] = value.astype(BF16)
-            remote(rsb.at[c, s, di], rrb.at[c, s, di], 4, ring_sem.at[0, c, s], at(MAIN, 1 if di == 0 else nz - 1))
+            remote(rsb.at[c, s, di], rrb.at[c, s, di], 4, ring_sem.at[c, s], at(MAIN, 1 if di == 0 else nz - 1))
 
         def spread(c, di, s):
             block = unit[c * nz + (zs[nz - s if s else 0] if di == 0 else zs[s])]
-            remote(block, block, 5, ring_sem.at[1, c, s], at(MAIN, 1 if di == 0 else nz - 1))
+            remote(block, block, 5, ring_sem.at[c, s], at(MAIN, 1 if di == 0 else nz - 1))
 
         def prepare(c, s):
             blocks = [target(c, di, s) for di in active(c, s)]
@@ -239,10 +251,11 @@
             for di, value in zip(active(c, 0), partials([target(c, di, 0) for di in active(c, 0)], c)):
                 pass_on(c, di, 0, value)
             prepare(c, 1)
+        pl.semaphore_signal(reach_sem.at[lm - 1], inc=1, device_id=at(HELPER), device_id_type=MESH)
         send_down(MAIN)
         for s in range(1, lm + 1):
             for c in ORDER:
-                arrived(rrb.at[c, 0, 0 : len(active(c, s - 1))], ring_sem.at[0, c, s - 1])
+                arrived(rrb.at[c, 0, 0 : len(active(c, s - 1))], ring_sem.at[c, s - 1])
                 if s < lm:
                     for di in active(c, s):
                         pass_on(c, di, s, pbuf[c, di] + rrb[c, s - 1, di].astype(F32))
@@ -284,7 +297,7 @@
             if s == 2:
                 arrived(unit[0 : NC * (nx - 1) * 2 + NC], one_sem.at[4])
             for c in ORDER:
-                arrived(unit[0 : len(active(c, s - 1))], ring_sem.at[1, c, s - 1])
+                arrived(unit[0 : len(active(c, s - 1))], ring_sem.at[c, s - 1])
                 for di in active(c, s):
                     spread(c, di, s)
                 if s > 1:
@@ -303,9 +316,7 @@
         for dj, dx in pairs:
             total = total + rb[dj, dx].astype(F32)
         total = total.reshape(tokens, width)
-        sums = jnp.sum(total, axis=1, keepdims=True)
-        apart = total - sums / width
-        st2[0] = columns_to_rows(sums, jnp.sum(apart * apart, axis=1, keepdims=True))
+        st2[0] = of_shard(total)
         tot[...] = total
         for core in (MAIN, HELPER):
             for dz in FAR:
@@ -329,6 +340,7 @@
             (7, unit[0 : 2 * len(pairs)]),
             (9, st1.at[1:nz]),
             (10, st2.at[1 : 2 * nz * nx]),
+            (11, st0.at[1 : 2 * nx]),
         ):
             arrived(ref, send_sem.at[group])
 
@@ -357,6 +369,7 @@
             pltpu.VMEM(row, F32),
             pltpu.VMEM((NC, depth, cw), BF16),
             pltpu.VMEM((fc, depth), BF16),
+            pltpu.VMEM((2 * nx, 2, tokens), F32),
             pltpu.VMEM((nz, 2, 2, tokens), F32),
             pltpu.VMEM((nz, rows, depth), BF16),
             pltpu.VMEM((NC, 3, rows, cw), F32),
@@ -369,11 +382,11 @@
             pltpu.VMEM((2 * nz * nx, 2, tokens), F32),
             pltpu.VMEM((tokens, width), F32),
             dma((3,)),
-            dma((11,)),
+            dma((12,)),
             dma((2, NC)),
-            dma((9,)),
-            dma((2, NC, nq)),
-            pltpu.SemaphoreType.REGULAR((nq - 1,)),
+            dma((10,)),
+            dma((NC, nq)),
+            pltpu.SemaphoreType.REGULAR((nq,)),
         ],
         compiler_params=pltpu.CompilerParams(collective_id=0, has_side_effects=True),
     )(

time: 57.4 us -> 55.1 us (0.960)
  Pallas kernels: 56.6 us -> 54.4 us
    pallas_call x1, Pallas kernels: 56.6 us -> 54.4 us  [per_device(): pl.pallas_call(functools.partial(kernel, nz, nx), out_shape=pltpu.VMEM((t...]
where the time goes in v6:
time: 55.1 us
  Pallas kernels  54.4 us (99%)
  local copies, waits for them, and re-layouts  0.63 us (1%)
    pallas_call x1, Pallas kernels, per_device(): pl.pallas_call(functools.partial(kernel, nz, nx), out_shape=pltpu.VMEM((t...  54.4 us

profile of v6, /device:TPU:1, one launch (start us, length us, event | category | flops | bytes accessed | tf_op | source)
XLA Modules:
  0.0 55.1 jit_solution(4844026196747192356)
XLA Ops:
  0.0 54.4 %shard_map.73 = bf16[256,128]{1,0:T(8,128)(2,1)S(1)} custom-call(bf16[256,128]{1,0:T(8,128)(2,1)} %res_hbm.1, f32[1,128]{1,0:T(1,128)} %bitcast.4, f32[1,128]{1,0:T(1,128)} %bitcast.5, bf16[128,8192]{1,0:T(8,128)(2,1)} %up_hbm.1, bf16[8192,128]{1,0:T(8,128)(2,1)} %dn_hbm.1, f32[1,128]{1,0:T(1,128)} %bitcast.6, f32[1,128]{1,0:T(1,128)} %bitcast.7), custom_call_target="tpu_custom_call" | custom-call | tf_op jit(solution)/shard_map/pallas_call | solution.py:359
  54.4 0.6 %copy.9 = bf16[256,128]{1,0:T(8,128)(2,1)} copy(bf16[256,128]{1,0:T(8,128)(2,1)S(1)} %shard_map.73) | data formatting | bytes 131072

commit v7 on v6

--- a/solution.py
+++ b/solution.py
@@ -11,7 +11,7 @@
 CB = ("cb_0", "cb_1")
 MESH = pl.DeviceIdType.MESH
 NC = 8
-ORDER = (0, 1, 2, 3, 4, 5, 6, 7)
+ORDER = (0, 5, 1, 3, 6, 2, 7, 4)
 FORWARDED = (0, 1, 2, 4)
 EARLY = (0, 1, 2)
 FAR = (4, 3, 5, 2, 6, 1, 7, 0)
@@ -58,7 +58,7 @@
 def kernel(
     nz, nx, res_hbm, gi_hbm, si_hbm, up_hbm, dn_hbm, go_hbm, so_hbm, out_ref,
     raw, gi, si, go, so, wup, wdn, st0, st1, normed, pbuf, rsb, rrb, hid, acc, sb, rb, st2, tot,
-    local_sem, send_sem, up_sem, one_sem, ring_sem, reach_sem,
+    local_sem, send_sem, raw_sem, up_sem, one_sem, ring_sem, reach_sem,
 ):
     tokens, width = res_hbm.shape
     nq = nz // 2
@@ -147,8 +147,16 @@
         greeted = enter([(MAIN, z, x, yw), at(MAIN)] + [at(core, 0, dx) for dx in range(1, nx) for core in (0, 1)])
         pltpu.make_async_copy(go_hbm, go, local_sem.at[1]).start()
         pltpu.make_async_copy(so_hbm, so, local_sem.at[1]).start()
+        early = [(c, dx) for c in EARLY for dx in (2, 1, 3)]
+        part = pl.ds(pl.multiple_of(w * hw, hw), hw)
+        for i, (c, dx) in enumerate(early):
+            pltpu.make_async_copy(up_hbm.at[part, up_cols(c, xs[dx])], unit[i], local_sem.at[0]).start()
+        arrived(unit[0 : len(early)], local_sem.at[0])
         greeted()
-        send_up(HELPER, EARLY)
+        for i, (c, dx) in enumerate(early):
+            remote(unit[i], wup.at[c, up_rows(x, w), :], 2, up_sem.at[0, c], at(HELPER, 0, dx))
+        for c in EARLY:
+            remote(up_hbm.at[:, up_cols(c, x)], wup.at[c, own, :], 2, up_sem.at[1, c], at(MAIN))
         for c in FORWARDED:
             arrived(unit[0 : nx - 1], up_sem.at[0, c])
             for dx in range(1, nx):
@@ -189,12 +197,14 @@
 
         for dj, dx in pairs:
             remote(st0.at[0], st0.at[dj * nx + dx], 11, one_sem.at[9], (MAIN, z, xs[dx], ys[dj]))
-        for dj, dx in pairs:
-            remote(raw.at[x, q], raw.at[x, q], 0, one_sem.at[2 + dj], (MAIN, z, xs[dx], ys[dj]))
+        for dx in (2, 1, 3):
+            remote(raw.at[x, q], raw.at[x, q], 0, raw_sem.at[dx], at(MAIN, 0, dx))
+        mate = (MAIN, z, x, ys[1])
+        remote(raw.at[x, q], raw.at[x, q], 0, raw_sem.at[0], mate)
         for dx in range(1, nx):
             remote(gi.at[x], gi.at[x], 1, one_sem.at[0], at(MAIN, 0, dx))
             remote(si.at[x], si.at[x], 8, one_sem.at[1], at(MAIN, 0, dx))
-        send_up(MAIN, ORDER)
+        send_up(MAIN, range(NC))
 
         for k in range(lm - 1):
             for dz in (1, nz - 1):
@@ -206,10 +216,13 @@
             st1[z, qs[dj]] = jnp.concatenate(pool(st0[dj * nx : (dj + 1) * nx], width), axis=0)
         for dz in FAR[:-1]:
             remote(st1.at[z], st1.at[z], 9, one_sem.at[8], at(MAIN, dz))
+        for dx in (1, 3, 2):
+            block = raw.at[xs[nx - dx], q]
+            arrived(block, raw_sem.at[dx])
+            remote(block, block, 0, raw_sem.at[0], mate)
         arrived(gi.at[1:nx], one_sem.at[0])
         arrived(si.at[1:nx], one_sem.at[1])
-        for dj in range(2):
-            arrived(unit[0 : 2 * (nx - 1 + dj)], one_sem.at[2 + dj])
+        arrived(unit[0 : 2 * nx], raw_sem.at[0])
         arrived(st1.at[1:nz], one_sem.at[8])
         for j in range(2):
             mean, scale = combine(st1[:, j], depth)
@@ -218,17 +231,17 @@
                 v = (raw[k, j].astype(F32) - mean) * scale * gi[k] + si[k]
                 normed[j * nq : (j + 1) * nq, :, k * width : (k + 1) * width] = v.astype(BF16).reshape(nq, rows, width)
 
-        def partials(blocks, c):
-            left = jnp.concatenate([normed[d] for d in blocks], axis=0)
-            both = jnp.dot(left, wup[c], preferred_element_type=F32)
-            return [both[i * rows : (i + 1) * rows] for i in range(len(blocks))]
+        def products(ks, c):
+            left = jnp.concatenate([normed[zs[k]] for k in ks], axis=0)
+            value = jnp.dot(left, wup[c], preferred_element_type=F32)
+            return [value[i * rows : (i + 1) * rows] for i in range(len(ks))]
 
         def active(c, s):
             return [di for di in range(2) if s < hops(c, di, nz)]
 
         def target(c, di, s):
             ahead = hops(c, di, nz) - s
-            return zs[ahead] if di == 0 else zs[nz - ahead]
+            return ahead if di == 0 else nz - ahead
 
         def pass_on(c, di, s, value):
             rsb[c, s, di] = value.astype(BF16)
@@ -238,19 +251,14 @@
             block = unit[c * nz + (zs[nz - s if s else 0] if di == 0 else zs[s])]
             remote(block, block, 5, ring_sem.at[c, s], at(MAIN, 1 if di == 0 else nz - 1))
 
-        def prepare(c, s):
-            blocks = [target(c, di, s) for di in active(c, s)]
-            if s == lm - 1:
-                blocks.append(z)
-            for slot, value in zip(active(c, s) + [2], partials(blocks, c)):
-                pbuf[c, slot] = value
-
         arrived(unit[0 : 2 * NC], local_sem.at[2])
         for c in ORDER:
             arrived(unit[0 : 2 * (nx - 1) + (2 if c < NC // 2 else 0)], up_sem.at[1, c])
-            for di, value in zip(active(c, 0), partials([target(c, di, 0) for di in active(c, 0)], c)):
-                pass_on(c, di, 0, value)
-            prepare(c, 1)
+            near = [target(c, di, s) for s in range(2) for di in range(2)]
+            values = products(near, c)
+            for di in range(2):
+                pass_on(c, di, 0, values[di])
+                pbuf[c, near[2 + di]] = values[2 + di]
         pl.semaphore_signal(reach_sem.at[lm - 1], inc=1, device_id=at(HELPER), device_id_type=MESH)
         send_down(MAIN)
         for s in range(1, lm + 1):
@@ -258,11 +266,13 @@
                 arrived(rrb.at[c, 0, 0 : len(active(c, s - 1))], ring_sem.at[c, s - 1])
                 if s < lm:
                     for di in active(c, s):
-                        pass_on(c, di, s, pbuf[c, di] + rrb[c, s - 1, di].astype(F32))
-                    if s < lm - 1:
-                        prepare(c, s + 1)
+                        pass_on(c, di, s, pbuf[c, target(c, di, s)] + rrb[c, s - 1, di].astype(F32))
+                    if s == 1:
+                        far = [target(c, di, t) for t in range(2, lm) for di in active(c, t)] + [0]
+                        for k, value in zip(far, products(far, c)):
+                            pbuf[c, k] = value
                 else:
-                    value = pbuf[c, 2]
+                    value = pbuf[c, 0]
                     for di in range(2):
                         value = value + rrb[c, hops(c, di, nz) - 1, di].astype(F32)
                     hid[c * nz + z] = jnp.square(jnp.maximum(value, 0.0)).astype(BF16)
@@ -270,11 +280,16 @@
                         spread(c, di, 0)
 
         def down(c, ks):
-            left = jnp.concatenate([hid[c * nz + zs[k]] for k in ks], axis=0)
-            value = jnp.dot(left, wdn[c * cw : (c + 1) * cw, :], preferred_element_type=F32)
+            place = ORDER.index(c)
+            if place % 2 == 0:
+                return
+            pair = (ORDER[place - 1], c)
+            halves = [jnp.concatenate([hid[half * nz + zs[k]] for k in ks], axis=0) for half in pair]
+            right = jnp.concatenate([wdn[half * cw : (half + 1) * cw, :] for half in pair], axis=0)
+            value = jnp.dot(jnp.concatenate(halves, axis=1), right, preferred_element_type=F32)
             for i, k in enumerate(ks):
                 part = value[i * rows : (i + 1) * rows]
-                acc[k] = part if c == ORDER[0] else acc[k] + part
+                acc[k] = part if place == 1 else acc[k] + part
 
         def branch(ks):
             for k in ks:
@@ -372,7 +387,7 @@
             pltpu.VMEM((2 * nx, 2, tokens), F32),
             pltpu.VMEM((nz, 2, 2, tokens), F32),
             pltpu.VMEM((nz, rows, depth), BF16),
-            pltpu.VMEM((NC, 3, rows, cw), F32),
+            pltpu.VMEM((NC, nz, rows, cw), F32),
             pltpu.VMEM((NC, nq, 2, rows, cw), BF16),
             pltpu.VMEM((NC, nq, 2, rows, cw), BF16),
             pltpu.VMEM((NC * nz, rows, cw), BF16),
@@ -383,6 +398,7 @@
             pltpu.VMEM((tokens, width), F32),
             dma((3,)),
             dma((12,)),
+            dma((nx,)),
             dma((2, NC)),
             dma((10,)),
             dma((NC, nq)),

time: 55.1 us -> 53.8 us (0.976)
  Pallas kernels: 54.4 us -> 53 us
    pallas_call x1, Pallas kernels: 54.4 us -> 53 us  [per_device(): pl.pallas_call(functools.partial(kernel, nz, nx), out_shape=pltpu.VMEM((t...]
where the time goes in v7:
time: 53.8 us; the launch traced here: 53.6 us
  Pallas kernels  53 us (99%)
  local copies, waits for them, and re-layouts  0.63 us (1%)
    pallas_call x1, Pallas kernels, per_device(): pl.pallas_call(functools.partial(kernel, nz, nx), out_shape=pltpu.VMEM((t...  53 us

profile of v7, /device:TPU:1, one launch (start us, length us, event | category | flops | bytes accessed | tf_op | source)
XLA Modules:
  0.0 53.6 jit_solution(11729622536041390563)
XLA Ops:
  0.0 53.0 %shard_map.73 = bf16[256,128]{1,0:T(8,128)(2,1)S(1)} custom-call(bf16[256,128]{1,0:T(8,128)(2,1)} %res_hbm.1, f32[1,128]{1,0:T(1,128)} %bitcast.4, f32[1,128]{1,0:T(1,128)} %bitcast.5, bf16[128,8192]{1,0:T(8,128)(2,1)} %up_hbm.1, bf16[8192,128]{1,0:T(8,128)(2,1)} %dn_hbm.1, f32[1,128]{1,0:T(1,128)} %bitcast.6, f32[1,128]{1,0:T(1,128)} %bitcast.7), custom_call_target="tpu_custom_call" | custom-call | tf_op jit(solution)/shard_map/pallas_call | solution.py:374
  53.0 0.6 %copy.9 = bf16[256,128]{1,0:T(8,128)(2,1)} copy(bf16[256,128]{1,0:T(8,128)(2,1)S(1)} %shard_map.73) | data formatting | bytes 131072

commit v8 on v7

--- a/solution.py
+++ b/solution.py
@@ -11,8 +11,8 @@
 CB = ("cb_0", "cb_1")
 MESH = pl.DeviceIdType.MESH
 NC = 8
-ORDER = (0, 5, 1, 3, 6, 2, 7, 4)
-FORWARDED = (0, 1, 2, 4)
+ORDER = (0, 5, 1, 6, 4, 3, 2, 7)
+FORWARDED = (0, 1, 4, 2)
 EARLY = (0, 1, 2)
 FAR = (4, 3, 5, 2, 6, 1, 7, 0)
 MAIN, HELPER = 1, 0
@@ -197,8 +197,11 @@
 
         for dj, dx in pairs:
             remote(st0.at[0], st0.at[dj * nx + dx], 11, one_sem.at[9], (MAIN, z, xs[dx], ys[dj]))
-        for dx in (2, 1, 3):
-            remote(raw.at[x, q], raw.at[x, q], 0, raw_sem.at[dx], at(MAIN, 0, dx))
+        halves = [slice(part * tokens // 2, (part + 1) * tokens // 2) for part in range(2)]
+        for part, place in enumerate(halves):
+            for dx in (2, 1, 3):
+                block = raw.at[x, q, place, :]
+                remote(block, block, 0, raw_sem.at[2 * dx + part], at(MAIN, 0, dx))
         mate = (MAIN, z, x, ys[1])
         remote(raw.at[x, q], raw.at[x, q], 0, raw_sem.at[0], mate)
         for dx in range(1, nx):
@@ -216,10 +219,11 @@
             st1[z, qs[dj]] = jnp.concatenate(pool(st0[dj * nx : (dj + 1) * nx], width), axis=0)
         for dz in FAR[:-1]:
             remote(st1.at[z], st1.at[z], 9, one_sem.at[8], at(MAIN, dz))
-        for dx in (1, 3, 2):
-            block = raw.at[xs[nx - dx], q]
-            arrived(block, raw_sem.at[dx])
-            remote(block, block, 0, raw_sem.at[0], mate)
+        for part, place in enumerate(halves):
+            for dx in (1, 3, 2):
+                block = raw.at[xs[nx - dx], q, place, :]
+                arrived(block, raw_sem.at[2 * dx + part])
+                remote(block, block, 0, raw_sem.at[0], mate)
         arrived(gi.at[1:nx], one_sem.at[0])
         arrived(si.at[1:nx], one_sem.at[1])
         arrived(unit[0 : 2 * nx], raw_sem.at[0])
@@ -398,7 +402,7 @@
             pltpu.VMEM((tokens, width), F32),
             dma((3,)),
             dma((12,)),
-            dma((nx,)),
+            dma((2 * nx,)),
             dma((2, NC)),
             dma((10,)),
             dma((NC, nq)),

time: 53.8 us -> 53.6 us (level)
  no operation moved by 1% of the time
where the time goes in v8:
time: 53.6 us; the launch traced here: 53.4 us
  Pallas kernels  52.8 us (99%)
  local copies, waits for them, and re-layouts  0.63 us (1%)
    pallas_call x1, Pallas kernels, per_device(): pl.pallas_call(functools.partial(kernel, nz, nx), out_shape=pltpu.VMEM((t...  52.8 us

profile of v8, /device:TPU:1, one launch (start us, length us, event | category | flops | bytes accessed | tf_op | source)
XLA Modules:
  0.0 53.4 jit_solution(8049482583826285019)
XLA Ops:
  0.0 52.8 %shard_map.73 = bf16[256,128]{1,0:T(8,128)(2,1)S(1)} custom-call(bf16[256,128]{1,0:T(8,128)(2,1)} %res_hbm.1, f32[1,128]{1,0:T(1,128)} %bitcast.4, f32[1,128]{1,0:T(1,128)} %bitcast.5, bf16[128,8192]{1,0:T(8,128)(2,1)} %up_hbm.1, bf16[8192,128]{1,0:T(8,128)(2,1)} %dn_hbm.1, f32[1,128]{1,0:T(1,128)} %bitcast.6, f32[1,128]{1,0:T(1,128)} %bitcast.7), custom_call_target="tpu_custom_call" | custom-call | tf_op jit(solution)/shard_map/pallas_call | solution.py:378
  52.8 0.6 %copy.9 = bf16[256,128]{1,0:T(8,128)(2,1)} copy(bf16[256,128]{1,0:T(8,128)(2,1)S(1)} %shard_map.73) | data formatting | bytes 131072

commit v9 on v8

--- a/solution.py
+++ b/solution.py
@@ -123,12 +123,12 @@
                     if c in FORWARDED:
                         part = pl.ds(pl.multiple_of(w * hw, hw), hw)
                         dst = wup.at[c, up_rows(x, w), :]
-                        remote(up_hbm.at[part, up_cols(c, xs[dx])], dst, 2, up_sem.at[0, c], at(HELPER, 0, dx))
+                        remote(up_hbm.at[part, up_cols(c, xs[dx])], dst, 2, up_sem.at[NC + FORWARDED.index(c)], at(HELPER, 0, dx))
                     else:
                         dst = wup.at[c, own, :]
-                        remote(up_hbm.at[:, up_cols(c, xs[dx])], dst, 2, up_sem.at[1, c], at(MAIN, 0, dx))
+                        remote(up_hbm.at[:, up_cols(c, xs[dx])], dst, 2, up_sem.at[c], at(MAIN, 0, dx))
                 if core == HELPER:
-                    remote(up_hbm.at[:, up_cols(c, x)], wup.at[c, own, :], 2, up_sem.at[1, c], at(MAIN))
+                    remote(up_hbm.at[:, up_cols(c, x)], wup.at[c, own, :], 2, up_sem.at[c], at(MAIN))
 
     def up_units(core):
         return sum((nx - 1) * (1 if c in FORWARDED else 2) for c in ORDER if c // (NC // 2) == core)
@@ -154,17 +154,17 @@
         arrived(unit[0 : len(early)], local_sem.at[0])
         greeted()
         for i, (c, dx) in enumerate(early):
-            remote(unit[i], wup.at[c, up_rows(x, w), :], 2, up_sem.at[0, c], at(HELPER, 0, dx))
+            remote(unit[i], wup.at[c, up_rows(x, w), :], 2, up_sem.at[NC + FORWARDED.index(c)], at(HELPER, 0, dx))
         for c in EARLY:
-            remote(up_hbm.at[:, up_cols(c, x)], wup.at[c, own, :], 2, up_sem.at[1, c], at(MAIN))
+            remote(up_hbm.at[:, up_cols(c, x)], wup.at[c, own, :], 2, up_sem.at[c], at(MAIN))
         for c in FORWARDED:
-            arrived(unit[0 : nx - 1], up_sem.at[0, c])
+            arrived(unit[0 : nx - 1], up_sem.at[NC + FORWARDED.index(c)])
             for dx in range(1, nx):
                 block = wup.at[c, up_rows(xs[dx], w), :]
-                remote(block, block, 3, up_sem.at[1, c], (MAIN, z, x, yw))
+                remote(block, block, 3, up_sem.at[c], (MAIN, z, x, yw))
             for dx in range(1, nx):
                 block = wup.at[c, up_rows(xs[dx], w), :]
-                remote(block, block, 3, up_sem.at[1, c], at(MAIN))
+                remote(block, block, 3, up_sem.at[c], at(MAIN))
             if c == FORWARDED[0]:
                 send_up(HELPER, [c for c in ORDER if c not in EARLY])
         pl.semaphore_wait(reach_sem.at[lm - 1], 1)
@@ -196,7 +196,7 @@
         greeted()
 
         for dj, dx in pairs:
-            remote(st0.at[0], st0.at[dj * nx + dx], 11, one_sem.at[9], (MAIN, z, xs[dx], ys[dj]))
+            remote(st0.at[0], st0.at[dj * nx + dx], 11, one_sem.at[3], (MAIN, z, xs[dx], ys[dj]))
         halves = [slice(part * tokens // 2, (part + 1) * tokens // 2) for part in range(2)]
         for part, place in enumerate(halves):
             for dx in (2, 1, 3):
@@ -214,11 +214,11 @@
                 pl.semaphore_signal(reach_sem.at[k], inc=1, device_id=at(MAIN, dz), device_id_type=MESH)
             pl.semaphore_wait(reach_sem.at[k], 2)
 
-        arrived(st0.at[1 : 2 * nx], one_sem.at[9])
+        arrived(st0.at[1 : 2 * nx], one_sem.at[3])
         for dj in range(2):
             st1[z, qs[dj]] = jnp.concatenate(pool(st0[dj * nx : (dj + 1) * nx], width), axis=0)
         for dz in FAR[:-1]:
-            remote(st1.at[z], st1.at[z], 9, one_sem.at[8], at(MAIN, dz))
+            remote(st1.at[z], st1.at[z], 9, one_sem.at[2], at(MAIN, dz))
         for part, place in enumerate(halves):
             for dx in (1, 3, 2):
                 block = raw.at[xs[nx - dx], q, place, :]
@@ -227,7 +227,7 @@
         arrived(gi.at[1:nx], one_sem.at[0])
         arrived(si.at[1:nx], one_sem.at[1])
         arrived(unit[0 : 2 * nx], raw_sem.at[0])
-        arrived(st1.at[1:nz], one_sem.at[8])
+        arrived(st1.at[1:nz], one_sem.at[2])
         for j in range(2):
             mean, scale = combine(st1[:, j], depth)
             mean, scale = row_to_lanes(mean), row_to_lanes(scale)
@@ -249,15 +249,15 @@
 
         def pass_on(c, di, s, value):
             rsb[c, s, di] = value.astype(BF16)
-            remote(rsb.at[c, s, di], rrb.at[c, s, di], 4, ring_sem.at[c, s], at(MAIN, 1 if di == 0 else nz - 1))
+            remote(rsb.at[c, s, di], rrb.at[c, s, di], 4, ring_sem.at[c, s % 2], at(MAIN, 1 if di == 0 else nz - 1))
 
         def spread(c, di, s):
             block = unit[c * nz + (zs[nz - s if s else 0] if di == 0 else zs[s])]
-            remote(block, block, 5, ring_sem.at[c, s], at(MAIN, 1 if di == 0 else nz - 1))
+            remote(block, block, 5, ring_sem.at[c, (s + 2) % 3], at(MAIN, 1 if di == 0 else nz - 1))
 
         arrived(unit[0 : 2 * NC], local_sem.at[2])
         for c in ORDER:
-            arrived(unit[0 : 2 * (nx - 1) + (2 if c < NC // 2 else 0)], up_sem.at[1, c])
+            arrived(unit[0 : 2 * (nx - 1) + (2 if c < NC // 2 else 0)], up_sem.at[c])
             near = [target(c, di, s) for s in range(2) for di in range(2)]
             values = products(near, c)
             for di in range(2):
@@ -267,7 +267,7 @@
         send_down(MAIN)
         for s in range(1, lm + 1):
             for c in ORDER:
-                arrived(rrb.at[c, 0, 0 : len(active(c, s - 1))], ring_sem.at[c, s - 1])
+                arrived(rrb.at[c, 0, 0 : len(active(c, s - 1))], ring_sem.at[c, (s - 1) % 2])
                 if s < lm:
                     for di in active(c, s):
                         pass_on(c, di, s, pbuf[c, target(c, di, s)] + rrb[c, s - 1, di].astype(F32))
@@ -316,7 +316,7 @@
             if s == 2:
                 arrived(unit[0 : NC * (nx - 1) * 2 + NC], one_sem.at[4])
             for c in ORDER:
-                arrived(unit[0 : len(active(c, s - 1))], ring_sem.at[c, s - 1])
+                arrived(unit[0 : len(active(c, s - 1))], ring_sem.at[c, (s + 1) % 3])
                 for di in active(c, s):
                     spread(c, di, s)
                 if s > 1:
@@ -403,9 +403,9 @@
             dma((3,)),
             dma((12,)),
             dma((2 * nx,)),
-            dma((2, NC)),
-            dma((10,)),
-            dma((NC, nq)),
+            dma((NC + len(FORWARDED),)),
+            dma((8,)),
+            dma((NC, 3)),
             pltpu.SemaphoreType.REGULAR((nq,)),
         ],
         compiler_params=pltpu.CompilerParams(collective_id=0, has_side_effects=True),

time: 53.6 us -> 53.5 us (level)
  no operation moved by 1% of the time
where the time goes in v9:
time: 53.5 us; the launch traced here: 53.3 us
  Pallas kernels  52.7 us (99%)
  local copies, waits for them, and re-layouts  0.63 us (1%)
    pallas_call x1, Pallas kernels, per_device(): pl.pallas_call(functools.partial(kernel, nz, nx), out_shape=pltpu.VMEM((t...  52.7 us

profile of v9, /device:TPU:1, one launch (start us, length us, event | category | flops | bytes accessed | tf_op | source)
XLA Modules:
  0.0 53.3 jit_solution(9067094541794970264)
XLA Ops:
  0.0 52.7 %shard_map.73 = bf16[256,128]{1,0:T(8,128)(2,1)S(1)} custom-call(bf16[256,128]{1,0:T(8,128)(2,1)} %res_hbm.1, f32[1,128]{1,0:T(1,128)} %bitcast.4, f32[1,128]{1,0:T(1,128)} %bitcast.5, bf16[128,8192]{1,0:T(8,128)(2,1)} %up_hbm.1, bf16[8192,128]{1,0:T(8,128)(2,1)} %dn_hbm.1, f32[1,128]{1,0:T(1,128)} %bitcast.6, f32[1,128]{1,0:T(1,128)} %bitcast.7), custom_call_target="tpu_custom_call" | custom-call | tf_op jit(solution)/shard_map/pallas_call | solution.py:378
  52.7 0.6 %copy.9 = bf16[256,128]{1,0:T(8,128)(2,1)} copy(bf16[256,128]{1,0:T(8,128)(2,1)S(1)} %shard_map.73) | data formatting | bytes 131072

commit v10 on v9

--- a/solution.py
+++ b/solution.py
@@ -161,10 +161,10 @@
             arrived(unit[0 : nx - 1], up_sem.at[NC + FORWARDED.index(c)])
             for dx in range(1, nx):
                 block = wup.at[c, up_rows(xs[dx], w), :]
-                remote(block, block, 3, up_sem.at[c], (MAIN, z, x, yw))
+                remote(block, block, 6, up_sem.at[c], (MAIN, z, x, yw))
             for dx in range(1, nx):
                 block = wup.at[c, up_rows(xs[dx], w), :]
-                remote(block, block, 3, up_sem.at[c], at(MAIN))
+                remote(block, block, 6, up_sem.at[c], at(MAIN))
             if c == FORWARDED[0]:
                 send_up(HELPER, [c for c in ORDER if c not in EARLY])
         pl.semaphore_wait(reach_sem.at[lm - 1], 1)
@@ -172,8 +172,7 @@
         remote(dn_hbm.at[pl.ds(share(x), fh), :], wdn.at[dn_rows(HELPER), own], 6, one_sem.at[4], at(MAIN))
         arrived(gi.at[0:2], local_sem.at[1])
         arrived(unit[0 : up_units(HELPER) + NC], send_sem.at[2])
-        arrived(unit[0 : 2 * (nx - 1) * len(FORWARDED)], send_sem.at[3])
-        arrived(unit[0 : nx * NC], send_sem.at[6])
+        arrived(unit[0 : 2 * (nx - 1) * len(FORWARDED) + nx * NC], send_sem.at[6])
         arrived(unit[0:4], one_sem.at[6])
         arrived(st2.at[0 : nz * nx], one_sem.at[7])
         finish()
@@ -196,14 +195,14 @@
         greeted()
 
         for dj, dx in pairs:
-            remote(st0.at[0], st0.at[dj * nx + dx], 11, one_sem.at[3], (MAIN, z, xs[dx], ys[dj]))
+            remote(st0.at[0], st0.at[dj * nx + dx], 0, one_sem.at[3], (MAIN, z, xs[dx], ys[dj]))
         halves = [slice(part * tokens // 2, (part + 1) * tokens // 2) for part in range(2)]
         for part, place in enumerate(halves):
             for dx in (2, 1, 3):
                 block = raw.at[x, q, place, :]
-                remote(block, block, 0, raw_sem.at[2 * dx + part], at(MAIN, 0, dx))
+                remote(block, block, 6, raw_sem.at[2 * dx + part], at(MAIN, 0, dx))
         mate = (MAIN, z, x, ys[1])
-        remote(raw.at[x, q], raw.at[x, q], 0, raw_sem.at[0], mate)
+        remote(raw.at[x, q], raw.at[x, q], 6, raw_sem.at[0], mate)
         for dx in range(1, nx):
             remote(gi.at[x], gi.at[x], 1, one_sem.at[0], at(MAIN, 0, dx))
             remote(si.at[x], si.at[x], 8, one_sem.at[1], at(MAIN, 0, dx))
@@ -218,12 +217,12 @@
         for dj in range(2):
             st1[z, qs[dj]] = jnp.concatenate(pool(st0[dj * nx : (dj + 1) * nx], width), axis=0)
         for dz in FAR[:-1]:
-            remote(st1.at[z], st1.at[z], 9, one_sem.at[2], at(MAIN, dz))
+            remote(st1.at[z], st1.at[z], 7, one_sem.at[2], at(MAIN, dz))
         for part, place in enumerate(halves):
             for dx in (1, 3, 2):
                 block = raw.at[xs[nx - dx], q, place, :]
                 arrived(block, raw_sem.at[2 * dx + part])
-                remote(block, block, 0, raw_sem.at[0], mate)
+                remote(block, block, 6, raw_sem.at[0], mate)
         arrived(gi.at[1:nx], one_sem.at[0])
         arrived(si.at[1:nx], one_sem.at[1])
         arrived(unit[0 : 2 * nx], raw_sem.at[0])
@@ -304,7 +303,7 @@
                 for dx in (2, 1, 3, 0):
                     cols = pl.ds(pl.multiple_of(xs[dx] * width, width), width)
                     send = functools.partial(
-                        remote, sb.at[o, :, cols], rb.at[dj, dx, i], 7, one_sem.at[5], (MAIN, z, xs[dx], y - q + j)
+                        remote, sb.at[o, :, cols], rb.at[dj, dx, i], 6, one_sem.at[5], (MAIN, z, xs[dx], y - q + j)
                     )
                     if dx:
                         send()
@@ -336,30 +335,28 @@
             total = total + rb[dj, dx].astype(F32)
         total = total.reshape(tokens, width)
         st2[0] = of_shard(total)
-        tot[...] = total
         for core in (MAIN, HELPER):
             for dz in FAR:
                 for dx in (2, 1, 3, 0):
                     k = dz * nx + dx
                     if k or core == HELPER:
-                        remote(st2.at[0], st2.at[k], 10, one_sem.at[7], at(core, dz, dx))
+                        remote(st2.at[0], st2.at[k], 3, one_sem.at[7], at(core, dz, dx))
             if core == MAIN:
-                remote(tot, tot, 0, one_sem.at[6], at(HELPER))
+                tot[...] = total
+                remote(tot, tot, 6, one_sem.at[6], at(HELPER))
         arrived(st2.at[1 : nz * nx], one_sem.at[7])
         finish()
 
         for group, ref in (
-            (0, unit[0 : 2 * len(pairs) + 4]),
             (1, gi.at[1:nx]),
             (8, si.at[1:nx]),
             (2, unit[0 : up_units(MAIN)]),
             (4, unit[0 : len(pairs) * NC]),
             (5, unit[0 : len(pairs) * NC]),
-            (6, unit[0 : (nx - 1) * NC]),
-            (7, unit[0 : 2 * len(pairs)]),
-            (9, st1.at[1:nz]),
-            (10, st2.at[1 : 2 * nz * nx]),
-            (11, st0.at[1 : 2 * nx]),
+            (6, unit[0 : (nx - 1) * NC + 4 * len(pairs) + 4]),
+            (7, st1.at[1:nz]),
+            (3, st2.at[1 : 2 * nz * nx]),
+            (0, st0.at[1 : 2 * nx]),
         ):
             arrived(ref, send_sem.at[group])
 
@@ -401,7 +398,7 @@
             pltpu.VMEM((2 * nz * nx, 2, tokens), F32),
             pltpu.VMEM((tokens, width), F32),
             dma((3,)),
-            dma((12,)),
+            dma((9,)),
             dma((2 * nx,)),
             dma((NC + len(FORWARDED),)),
             dma((8,)),

time: 53.5 us -> 53.4 us (level)
  no operation moved by 1% of the time
where the time goes in v10:
time: 53.4 us; the launch traced here: 53.3 us
  Pallas kernels  52.6 us (99%)
  local copies, waits for them, and re-layouts  0.63 us (1%)
    pallas_call x1, Pallas kernels, per_device(): pl.pallas_call(functools.partial(kernel, nz, nx), out_shape=pltpu.VMEM((t...  52.6 us

profile of v10, /device:TPU:1, one launch (start us, length us, event | category | flops | bytes accessed | tf_op | source)
XLA Modules:
  0.0 53.3 jit_solution(11281915155597024101)
XLA Ops:
  0.0 52.6 %shard_map.73 = bf16[256,128]{1,0:T(8,128)(2,1)S(1)} custom-call(bf16[256,128]{1,0:T(8,128)(2,1)} %res_hbm.1, f32[1,128]{1,0:T(1,128)} %bitcast.4, f32[1,128]{1,0:T(1,128)} %bitcast.5, bf16[128,8192]{1,0:T(8,128)(2,1)} %up_hbm.1, bf16[8192,128]{1,0:T(8,128)(2,1)} %dn_hbm.1, f32[1,128]{1,0:T(1,128)} %bitcast.6, f32[1,128]{1,0:T(1,128)} %bitcast.7), custom_call_target="tpu_custom_call" | custom-call | tf_op jit(solution)/shard_map/pallas_call | solution.py:375
  52.6 0.6 %copy.9 = bf16[256,128]{1,0:T(8,128)(2,1)} copy(bf16[256,128]{1,0:T(8,128)(2,1)S(1)} %shard_map.73) | data formatting | bytes 131072
